TPU v7x, 32 devices: a whole 2x2x4 slice. The times are simulated.
32 devices in a mesh: ep: 8 (over z, x), tp: 4 (over y, core).
Axes of the slice: x: 2, y: 2, z: 4, core: 2. Of those that a mesh axis runs over, the one named last changes fastest.
Arguments:
- initial_micro_probes: bfloat16 [2048, 2048], P('ep', 'tp'), may hold values from -6 to 6
- initial_micro_lookup_keys: bfloat16 [2048, 2048], P('ep', 'tp'), may hold values from -6 to 6
- initial_micro_payloads: bfloat16 [2048, 2048], P('ep', 'tp'), may hold values from -6 to 6
- result_switch_preactivation: bfloat16 [2048, 2048], P('ep', 'tp'), may hold values from -6 to 6
- insertion_power_preactivation: float32 [2048, 16], P('ep', 'tp'), may hold values from -6 to 6
- fading_preactivation: float32 [2048, 16], P('ep', 'tp'), may hold values from -4.5 to 4.5
- extra_fading_term: float32 [2048, 16], P('ep', 'tp'), may hold values from -0.7 to 0
- channel_fading_speed: float32 [16], P('tp'), may hold values from 2.4414063e-05 to 0.04
- result_scaling_vector: float32 [128], replicated, may hold values from 0.1 to 1.9
- result_mapping_weights: bfloat16 [2048, 2048], P('tp'), may hold values from -0.125 to 0.125
- latter_micro_entries: bfloat16 [1024, 2048], P('ep'), may hold values from -6 to 6
- specialist_scaling_vector: float32 [2048], replicated, may hold values from 0.1 to 1.9
- selected_specialists: int32 [1024, 2], P('ep'), may hold values from 0 to 7, all different within a row; in each aligned block of 128 rows (0 to 127, 128 to 255, ...) at most 64 rows name the same one
- selected_dispatch_weights: float32 [1024, 2], P('ep'), may hold values from 0.1 to 1
- specialist_switch_weights: bfloat16 [8, 2048, 4096], P('ep', None, 'tp'), may hold values from -0.125 to 0.125
- specialist_expand_weights: bfloat16 [8, 2048, 4096], P('ep', None, 'tp'), may hold values from -0.125 to 0.125
- specialist_contract_weights: bfloat16 [8, 4096, 2048], P('ep', 'tp'), may hold values from -0.09375 to 0.09375
Outputs:
- mixer_out: bfloat16 [2048, 2048], P(('ep', 'tp'))
- moe_out: bfloat16 [1024, 2048], P('ep')
Inputs may be any that keep to these rules, and one draw needn't show every extreme that they name: `selected_specialists`: each row names 2 different experts. Among the 128 rows of one index of ep no expert is named by more than 64 rows, a bound that some block reaches.
All inputs are finite; a program needn't handle non-finite values.
Results may differ from a plain program's by a relative error of at most 0.024.
Values may be sent and summed in bfloat16 or wider, within the bound.
A program may use at most 64 MiB of HBM per device.

v0:
```python
import jax
import jax.numpy as jnp
from jax import lax
from jax.sharding import PartitionSpec as P

BLK = 64


EPS = 1e-06


def carried_in(value, axis, combine, identity):
    length, mine = (lax.axis_size(axis), lax.axis_index(axis))
    everything = jax.tree.map(
        lambda part, kind: lax.all_gather(part.astype(kind), axis),
        value,
        (jnp.bfloat16, jnp.bfloat16),
    )
    start = jax.tree.map(
        lambda part, zero: jnp.broadcast_to(jnp.asarray(zero, part.dtype), part.shape),
        value,
        identity,
    )

    def turn(k, before):
        reached = k < mine
        new = combine(
            before, jax.tree.map(lambda part, own: part[k].astype(own.dtype), everything, value)
        )
        return jax.tree.map(lambda a, b: jnp.where(reached, a, b), new, before)

    return lax.fori_loop(0, length, turn, start)


def exact_product(left, right):
    return jnp.matmul(left, right, precision=lax.Precision.HIGHEST)


def flipped(matrix):
    return jnp.swapaxes(matrix, -1, -2)


def unit_length(values):
    wide = values.astype(jnp.float32)
    return wide * lax.rsqrt(jnp.sum(wide * wide, axis=-1, keepdims=True) + EPS)


def to_blocks(values, block_count):
    shaped = values.reshape(
        block_count, values.shape[0] // block_count, values.shape[1], values.shape[2]
    )
    return jnp.transpose(shaped, (0, 2, 1, 3))


def unit_inverse(lower):
    size = lower.shape[-1]
    identity = jnp.eye(size, dtype=jnp.float32)
    power = -lower
    result = identity + power
    reach = 2
    while reach < size:
        power = exact_product(power, power)
        result = exact_product(result, identity + power)
        reach = reach * 2
    return result


def block_terms(query, key, value, write, fading_exponent):
    size = query.shape[2]
    running = jnp.cumsum(fading_exponent, axis=-1)
    last = running[..., -1:]
    row_ids = lax.broadcasted_iota(jnp.int32, (size, size), 0)
    col_ids = lax.broadcasted_iota(jnp.int32, (size, size), 1)
    inclusive = row_ids >= col_ids
    strict = row_ids > col_ids
    spread = running[..., :, None] - running[..., None, :]
    fading = jnp.where(inclusive, jnp.exp(jnp.where(inclusive, spread, 0.0)), 0.0)
    key_write = key * write[..., None]
    lower = jnp.where(strict, exact_product(key_write, flipped(key)) * fading, 0.0)
    inverse = unit_inverse(lower)
    update = exact_product(inverse, value * write[..., None])
    erase = exact_product(inverse, key_write * jnp.exp(running)[..., None])
    scores = exact_product(query, flipped(key)) * fading
    query_fade = query * jnp.exp(running)[..., None]
    key_fade = key * jnp.exp(last - running)[..., None]
    return (update, erase, scores, query_fade, key_fade, jnp.exp(last))


def advance(state, inputs):
    update, erase, scores, query_fade, key_fade, block_fade = inputs
    fresh = update - exact_product(erase, state)
    reads = exact_product(query_fade, state) + exact_product(scores, fresh)
    state = state * block_fade[..., None] + exact_product(flipped(key_fade), fresh)
    return (state, reads)


def compose(carry, inputs):
    mapping, offset = carry
    update, erase, scores, query_fade, key_fade, block_fade = inputs
    across = flipped(key_fade)
    identity = jnp.eye(mapping.shape[-1], dtype=jnp.float32)
    step_map = block_fade[..., None] * identity - exact_product(across, erase)
    step_offset = exact_product(across, update)
    return ((exact_product(step_map, mapping), exact_product(step_map, offset) + step_offset), None)


def chain_maps(earlier, later):
    return (exact_product(later[0], earlier[0]), exact_product(later[0], earlier[1]) + later[1])


def gated_norm(reads, result_switch_preactivation, result_scaling_vector):
    row_count, head_count, value_width = reads.shape
    scale = lax.rsqrt(jnp.mean(reads * reads, axis=-1, keepdims=True) + EPS)
    gate = jax.nn.silu(
        result_switch_preactivation.reshape(row_count, head_count, value_width).astype(jnp.float32)
    )
    return (
        (reads * scale * result_scaling_vector * gate)
        .astype(jnp.bfloat16)
        .reshape(row_count, head_count * value_width)
    )


def slot_table(flat_route, picks, experts, capacity):
    chosen = (flat_route[:, None] == lax.broadcasted_iota(jnp.int32, (1, experts), 1)).astype(
        jnp.int32
    )
    earlier = jnp.cumsum(chosen, axis=0) - chosen
    position = jnp.sum(earlier * chosen, axis=1)
    source = lax.broadcasted_iota(jnp.int32, flat_route.shape, 0) // picks
    table = (
        jnp.full((capacity * experts,), -1, jnp.int32)
        .at[position * experts + flat_route]
        .set(source)
    )
    return (table.reshape(capacity, experts), position)


def fill_slots(table, normed_in):
    picked = normed_in[jnp.maximum(table, 0)]
    return jnp.where((table >= 0)[..., None], picked, jnp.zeros_like(picked))


def expert_hidden(rows_in, gate_weight, up_weight):
    gate = jnp.dot(rows_in, gate_weight, preferred_element_type=jnp.float32)
    upward = jnp.dot(rows_in, up_weight, preferred_element_type=jnp.float32)
    return (jax.nn.silu(gate) * upward).astype(jnp.bfloat16)


def local(
    initial_micro_probes,
    initial_micro_lookup_keys,
    initial_micro_payloads,
    result_switch_preactivation,
    insertion_power_preactivation,
    fading_preactivation,
    extra_fading_term,
    channel_fading_speed,
    result_scaling_vector,
    result_mapping_weights,
    latter_micro_entries,
    specialist_scaling_vector,
    selected_specialists,
    selected_dispatch_weights,
    specialist_switch_weights,
    specialist_expand_weights,
    specialist_contract_weights,
):
    groups = lax.axis_size("tp")
    row_count = initial_micro_probes.shape[0]
    head_count = channel_fading_speed.shape[0]
    key_width = initial_micro_probes.shape[1] // head_count
    value_width = initial_micro_payloads.shape[1] // head_count
    block_count = row_count // BLK
    query = to_blocks(
        unit_length(initial_micro_probes.reshape(row_count, head_count, key_width)), block_count
    )
    key = to_blocks(
        unit_length(initial_micro_lookup_keys.reshape(row_count, head_count, key_width)),
        block_count,
    )
    value = to_blocks(
        initial_micro_payloads.reshape(row_count, head_count, value_width).astype(jnp.float32),
        block_count,
    )
    write = to_blocks(jax.nn.sigmoid(insertion_power_preactivation)[..., None], block_count)[..., 0]
    fading_exponent = extra_fading_term - channel_fading_speed[None, :] * jax.nn.softplus(
        fading_preactivation
    )
    fading_exponent = to_blocks(fading_exponent[..., None], block_count)[..., 0]
    terms = block_terms(query, key, value, write, fading_exponent)
    identity = jnp.broadcast_to(
        jnp.eye(key_width, dtype=jnp.float32), (head_count, key_width, key_width)
    )
    empty = jnp.zeros((head_count, key_width, value_width), jnp.float32)
    (span_map, span_offset), unused = lax.scan(compose, (identity, empty), terms)
    prior = carried_in((span_map, span_offset), "ep", chain_maps, (identity, empty))
    final_state, reads = lax.scan(advance, prior[1], terms)
    reads = jnp.transpose(reads, (0, 2, 1, 3)).reshape(row_count, head_count, value_width)
    normed = gated_norm(reads, result_switch_preactivation, result_scaling_vector)
    mixer_out = lax.psum_scatter(
        jnp.dot(normed, result_mapping_weights, preferred_element_type=jnp.float32).astype(
            jnp.bfloat16
        ),
        "tp",
        scatter_dimension=0,
        tiled=True,
    )
    token_count = latter_micro_entries.shape[0]
    picks = selected_specialists.shape[1]
    experts = lax.axis_size("ep")
    capacity = 2 * token_count * picks // experts
    model_width = latter_micro_entries.shape[1]
    wide_in = latter_micro_entries.astype(jnp.float32)
    normed_in = (
        wide_in
        * lax.rsqrt(jnp.mean(wide_in * wide_in, axis=-1, keepdims=True) + EPS)
        * specialist_scaling_vector
    ).astype(jnp.bfloat16)
    flat_route = selected_specialists.reshape(-1)
    table, position = slot_table(flat_route, picks, experts, capacity)
    share_cap = capacity // groups
    own_table = lax.dynamic_slice_in_dim(table, lax.axis_index("tp") * share_cap, share_cap, 0)
    arrived = lax.all_to_all(
        fill_slots(own_table, normed_in), "ep", split_axis=1, concat_axis=1, tiled=True
    )
    piece = lax.all_gather(arrived, "tp", axis=0, tiled=True)
    flat_piece = piece.reshape(-1, model_width)
    result = expert_hidden(flat_piece, specialist_switch_weights[0], specialist_expand_weights[0])
    hidden = result.reshape(piece.shape[0], piece.shape[1], -1)
    hidden = hidden.reshape(-1, hidden.shape[-1])
    summed = lax.psum_scatter(
        jnp.dot(hidden, specialist_contract_weights[0], preferred_element_type=jnp.float32).astype(
            jnp.bfloat16
        ),
        "tp",
        scatter_dimension=0,
        tiled=True,
    ).astype(jnp.float32)
    summed = summed.astype(jnp.bfloat16).reshape(capacity // groups, experts, model_width)
    returned = lax.all_to_all(summed, "ep", split_axis=1, concat_axis=1, tiled=True)
    slots = lax.all_gather(returned, "tp", axis=0, tiled=True)
    values = slots[position, flat_route].reshape(token_count, picks, model_width)
    route_weight = selected_dispatch_weights / jnp.sum(
        selected_dispatch_weights, axis=1, keepdims=True
    )
    moe_out = jnp.sum(values.astype(jnp.float32) * route_weight[..., None], axis=1).astype(
        jnp.bfloat16
    )
    return (mixer_out, moe_out)


def solution(mesh):
    return jax.shard_map(
        local,
        mesh=mesh,
        in_specs=(
            P("ep", "tp"),
            P("ep", "tp"),
            P("ep", "tp"),
            P("ep", "tp"),
            P("ep", "tp"),
            P("ep", "tp"),
            P("ep", "tp"),
            P("tp"),
            P(),
            P("tp", None),
            P("ep", None),
            P(),
            P("ep", None),
            P("ep", None),
            P("ep", None, "tp"),
            P("ep", None, "tp"),
            P("ep", "tp", None),
        ),
        out_specs=(P(("ep", "tp"), None), P("ep", None)),
        check_vma=False,
    )
```

profile of v0, /device:TPU:0, one launch (start us, length us, event | category | flops | bytes accessed | tf_op | source)
XLA Modules:
  0.0 264.2 jit_solution(10858812635770844773)
XLA Ops:
  10.4 1.4 scatter_custom_fusion
  12.0 1.2 fusion.55
  13.3 1.2 fusion.57
  14.6 0.9 gather_fusion
  15.5 1.4 copy_select_fusion
  16.9 7.4 %all-to-all-start = ((bf16[16,8,2048]{2,0,1:T(8,128)(2,1)}), bf16[16,8,2048]{2,0,1:T(8,128)(2,1)}, u32[]{:S(2)}, u32[]{:S(2)}) async-start(bf16[16,8,2048]{2,0,1:T(8,128)(2,1)} %copy_select_fusion), calls=%async_computation.1 | async-start | bytes 1048576 | tf_op jit(solution)/shard_map/all_to_all | solution.py:224
  25.5 1.0 reshape.224
  26.7 0.9 reduce_window_sum.26
  29.3 2.0 mul.197
  31.3 1.4 reduce_sum.65
  32.7 1.0 mul.210
  33.7 1.4 reduce_sum.66
  35.9 1.9 reshape.226
  38.6 4.5 %broadcast_multiply_fusion = (f32[4,4,64,128]{3,1,2,0:T(4,128)}, f32[4,4,64,128]{3,1,2,0:T(4,128)}, f32[4,4,64,128]{3,1,2,0:T(4,128)}, f32[4,4,64,128]{3,1,2,0:T...) fusion(f32[4,4,64]{1,2,0:T(8,128)} %copy.113, f32[4,64,4,128]{3,2,1,0:T(4,128)S(1)} %copy-done.4, ...), kind=kLoop, calls=%fused_computation.110 | loop fusion | flops 917504 | bytes 4739072 | tf_op jit(solution)/shard_map/mul | solution.py:84
  43.1 1.1 copy.117
  45.1 1.3 multiply_bitcast_fusion.1
  47.2 2.0 fusion.54
  49.2 2.1 copy.133
  58.3 1.5 fusion.68
  59.8 1.5 fusion.70
  61.2 14.3 %all-gather.7.cloned.1.call-done = bf16[64,8,2048]{2,1,0:T(8,128)(2,1)} async-done(((bf16[16,8,2048]{2,1,0:T(8,128)(2,1)}), bf16[64,8,2048]{2,1,0:T(8,128)(2,1)}) %all-gather.7.cloned.1.call-update) | async-done | bytes 2097168 | tf_op jit(solution)/shard_map/all_gather | solution.py:227
  75.5 6.5 %fusion.42 = f32[512,1024]{1,0:T(8,128)} fusion(bf16[1,2048,1024]{2,1,0:T(8,128)(2,1)} %param.37, bf16[64,8,2048]{2,1,0:T(8,128)(2,1)} %all-gather.7.cloned.1.call-done), kind=kOutput, calls=%fused_computation.56 | convolution fusion | flops 2147483648 | bytes 8388608 | tf_op jit(solution)/shard_map/dot_general | solution.py:145
  82.0 10.8 %fusion.44 = bf16[512,2048]{1,0:T(8,128)(2,1)} fusion(bf16[1,1024,2048]{2,1,0:T(8,128)(2,1)} %param.39, f32[512,1024]{1,0:T(8,128)} %fusion.42, bf16[1,2048,1024]{2,1,0:T(8,128)(2,1)} %param.38, bf16[64,8,2048]{2,1,0:T(8,128)(2,1)} %all-gather.7.cloned.1.call-done), kind=kOutput, calls=%fused_computation.58 | convolution fusion | flops 4299161600 | bytes 14680064 | tf_op jit(solution)/shard_map/dot_general | solution.py:233
  92.9 15.7 %while.40 = (s32[]{:T(128)}, f32[4,128,128]{2,1,0:T(8,128)S(1)}, f32[4,128,128]{2,1,0:T(8,128)S(1)}, f32[4,4,1]{1,2,0:T(1,128)S(1)}, f32[4,4,64,128]{3,2,1,0:T(8...) while((s32[]{:T(128)}, f32[4,128,128]{2,1,0:T(8,128)S(1)}, ...), condition=%wide.region_3.4_spmd.clone, body=%wide.region_2.3_spmd.clone.sunk | while | flops 302284800 | bytes 3541643 | solution.py:196
  93.0 1.5 convolution_subtract_fusion.5
  94.9 1.5 convolution_add_fusion.8
  96.9 1.5 convolution_subtract_fusion.5
  98.8 1.5 convolution_add_fusion.8
  100.8 1.5 convolution_subtract_fusion.5
  102.7 1.5 convolution_add_fusion.8
  104.7 1.5 convolution_subtract_fusion.5
  106.6 1.5 convolution_add_fusion.8
  110.1 2.2 convolution_multiply_fusion
  112.3 11.9 %reduce-scatter.5.cloned.1.call-done = bf16[128,2048]{1,0:T(8,128)(2,1)} async-done(((bf16[512,2048]{1,0:T(8,128)(2,1)}), bf16[128,2048]{1,0:T(8,128)(2,1)}) %reduce-scatter.5.cloned.1.call-update) | async-done | bytes 524304 | tf_op jit(solution)/shard_map/reduce_scatter | solution.py:232
  124.2 2.1 copy.134
  126.3 5.5 %all-to-all-start.1 = ((bf16[16,8,2048]{2,0,1:T(8,128)(2,1)}), bf16[16,8,2048]{2,0,1:T(8,128)(2,1)}, u32[]{:S(2)}, u32[]{:S(2)}) async-start(bf16[16,8,2048]{2,0,1:T(8,128)(2,1)} %copy.134), calls=%async_computation.3 | async-start | bytes 1048576 | tf_op jit(solution)/shard_map/all_to_all | solution.py:241
  131.8 22.6 %all-gather.11.cloned.1.call-done = bf16[32,128,128]{2,1,0:T(8,128)(2,1)} async-done(((bf16[4,128,128]{2,1,0:T(8,128)(2,1)}), bf16[32,128,128]{2,1,0:T(8,128)(2,1)}) %all-gather.11.cloned.1.call-update) | async-done | bytes 1048592 | tf_op jit(solution)/shard_map/all_gather | solution.py:15
  154.4 40.7 %all-gather.13.cloned.1.call-done = bf16[32,128,128]{2,1,0:T(8,128)(2,1)} async-done(((bf16[4,128,128]{2,1,0:T(8,128)(2,1)}), bf16[32,128,128]{2,1,0:T(8,128)(2,1)}) %all-gather.13.cloned.1.call-update) | async-done | bytes 1048592 | tf_op jit(solution)/shard_map/all_gather | solution.py:15
  195.1 10.6 %while.41 = (s32[]{:T(128)}, f32[4,128,128]{2,1,0:T(8,128)S(1)}, s32[]{:T(128)}, bf16[8,4,128,128]{3,2,1,0:T(8,128)(2,1)}, bf16[8,4,128,128]{3,2,1,0:T(8,128)(2,1)}, /*index=5*/s32[]{:T(128)}, s32[]{:T(128)}) while((s32[]{:T(128)}, f32[4,128,128]{2,1,0:T(8,128)S(1)}, s32[]{:T(128)}, bf16[8,4,128,128]{3,2,1,0:T(8,128)(2,1)}, ...), condition=%wide.region_5.6_spmd.clone, body=%wide.region_4.5_spmd.clone.sunk | while | flops 100990976 | bytes 1575519 | solution.py:32
  195.1 1.3 fusion.189
  196.4 1.3 fusion.189
  197.8 1.3 fusion.189
  199.1 1.3 fusion.189
  200.4 1.3 fusion.189
  201.7 1.3 fusion.189
  203.1 1.3 fusion.189
  204.4 1.3 fusion.189
  205.7 2.1 copy.135
  207.9 16.9 %while.39 = (s32[]{:T(128)}, f32[4,128,128]{2,1,0:T(8,128)S(1)}, f32[4,4,64,128]{3,2,1,0:T(8,128)}, f32[4,4,1]{1,2,0:T(1,128)S(1)}, f32[4,4,64,128]{3,2,1,0:T(8,...) while((s32[]{:T(128)}, f32[4,128,128]{2,1,0:T(8,128)S(1)}, ...), condition=%wide.region_8.9_spmd, body=%wide.region_7.8_spmd.sunk | while | flops 176357376 | bytes 2754709 | solution.py:198
  207.9 1.3 convolution_subtract_fusion.4
  210.4 1.0 fusion.174
  212.1 1.4 convolution_subtract_fusion.4
  214.7 1.0 fusion.174
  216.3 1.3 convolution_subtract_fusion.4
  218.9 1.0 fusion.174
  220.5 1.3 convolution_subtract_fusion.4
  223.1 1.0 fusion.174
  224.8 1.3 multiply_reduce_fusion.1
  226.2 1.4 copy.125
  228.0 1.8 convolution_convert_fusion
  229.9 5.1 %gather_fusion.1 = bf16[256,2048]{1,0:T(8,128)(2,1)} fusion(bf16[64,8,2048]{2,1,0:T(8,128)(2,1)} %all-gather.9.cloned.1.call-done, s32[256]{0:T(256)S(1)} %bitcast.192), kind=kCustom, calls=%fused_computation.1 | custom fusion | bytes 2099200 | tf_op jit(solution)/shard_map/gather | solution.py:243
  235.0 3.4 %reshape.225 = f32[128,2,2048]{2,1,0:T(2,128)} reshape(bf16[256,2048]{1,0:T(8,128)(2,1)} %gather_fusion.1) | data formatting | bytes 3145728 | tf_op jit(solution)/shard_map/convert_element_type | solution.py:247
  238.4 5.7 %multiply_reduce_fusion = bf16[128,2048]{1,0:T(8,128)(2,1)} fusion(f32[128,2,2048]{2,1,0:T(2,128)} %reshape.225, f32[128,2]{1,0:T(8,128)S(1)} %copy.136), kind=kLoop, calls=%fused_computation.62 | loop fusion | flops 786432 | bytes 2622464 | tf_op jit(solution)/shard_map/reduce_sum | solution.py:247
  244.1 12.9 %reduce-scatter.3.cloned.1.call-done = bf16[64,2048]{1,0:T(8,128)(2,1)} async-done(((bf16[256,2048]{1,0:T(8,128)(2,1)}), bf16[64,2048]{1,0:T(8,128)(2,1)}) %reduce-scatter.3.cloned.1.call-update) | async-done | bytes 262160 | tf_op jit(solution)/shard_map/reduce_scatter | solution.py:201
  (147 shorter events, 28.6 us)
Async XLA Ops:
  8.0 219.9 %copy-start = (bf16[512,2048]{1,0:T(8,128)(2,1)S(1)}, bf16[512,2048]{1,0:T(8,128)(2,1)}, u32[]{:S(2)}) copy-start(bf16[512,2048]{1,0:T(8,128)(2,1)} %param.32) | copy-start | bytes 6291460
  15.5 8.9 %copy-start.6 = (bf16[256,512]{1,0:T(8,128)(2,1)S(1)}, bf16[256,512]{1,0:T(8,128)(2,1)}, u32[]{:S(2)}) copy-start(bf16[256,512]{1,0:T(8,128)(2,1)} %param.24) | copy-start | bytes 786436
  15.5 10.0 %copy-start.7 = (bf16[256,512]{1,0:T(8,128)(2,1)S(1)}, bf16[256,512]{1,0:T(8,128)(2,1)}, u32[]{:S(2)}) copy-start(bf16[256,512]{1,0:T(8,128)(2,1)} %param.23) | copy-start | bytes 786436
  16.9 9.6 %copy-start.8 = (f32[256,4]{0,1:T(4,128)S(1)}, f32[256,4]{0,1:T(4,128)}, u32[]{:S(2)}) copy-start(f32[256,4]{0,1:T(4,128)} %param.29) | copy-start | bytes 12292
  16.9 9.6 %copy-start.9 = (f32[256,4]{0,1:T(4,128)S(1)}, f32[256,4]{0,1:T(4,128)}, u32[]{:S(2)}) copy-start(f32[256,4]{0,1:T(4,128)} %param.28) | copy-start | bytes 12292
  16.9 9.6 %copy-start.11 = (f32[4]{0:T(128)S(1)}, f32[4]{0:T(128)}, u32[]{:S(2)}) copy-start(f32[4]{0:T(128)} %param.30) | copy-start | bytes 52
  16.9 32.3 %all-to-all-start = ((bf16[16,8,2048]{2,0,1:T(8,128)(2,1)}), bf16[16,8,2048]{2,0,1:T(8,128)(2,1)}, u32[]{:S(2)}, u32[]{:S(2)}) async-start(bf16[16,8,2048]{2,0,1:T(8,128)(2,1)} %copy_select_fusion), calls=%async_computation.1 | async-start | bytes 1048576 | tf_op jit(solution)/shard_map/all_to_all | solution.py:224
  24.4 51.1 %all-gather.7.cloned.1.call-start = ((), (), s32[]{:S(2)}) async-start(), calls=%async_computation.5 | async-start | bytes 2621440 | tf_op jit(solution)/shard_map/all_gather | solution.py:227
  32.7 5.9 %copy-start.5 = (f32[256,4]{1,0:T(8,128)}, f32[256,4]{1,0:T(8,128)S(1)}, u32[]{:S(2)}) copy-start(f32[256,4]{1,0:T(8,128)S(1)} %add_rsqrt_fusion.1) | copy-start | bytes 12292
  33.7 4.9 %copy-start.4 = (f32[4,64,4,128]{3,2,1,0:T(4,128)S(1)}, f32[4,64,4,128]{3,2,1,0:T(4,128)}, u32[]{:S(2)}) copy-start(f32[4,64,4,128]{3,2,1,0:T(4,128)} %reshape.224) | copy-start | bytes 1572868
  46.3 0.8 copy-start.1
  51.4 72.8 %reduce-scatter.5.cloned.1.call-start = ((), (), s32[]{:S(2)}) async-start(), calls=%async_computation.6 | async-start | bytes 2621440 | tf_op jit(solution)/shard_map/reduce_scatter | solution.py:232
  56.3 2.0 copy-start.3
  57.0 2.8 %copy-start.2 = (f32[4,4,64,128]{3,1,2,0:T(4,128)S(1)}, f32[4,4,64,128]{3,1,2,0:T(4,128)}, u32[]{:S(2)}) copy-start(f32[4,4,64,128]{3,1,2,0:T(4,128)} %get-tuple-element.355) | copy-start | bytes 1572868
  92.8 61.6 %all-gather.11.cloned.1.call-start = ((), (), s32[]{:S(2)}) async-start(), calls=%async_computation.8 | async-start | bytes 1179648 | tf_op jit(solution)/shard_map/all_gather | solution.py:15
  92.9 17.2 %copy-start.12 = (f32[128]{0:T(128)S(1)}, f32[128]{0:T(128)}, u32[]{:S(2)}) copy-start(f32[128]{0:T(128)} %param.31) | copy-start | bytes 1540
  109.3 85.8 %all-gather.13.cloned.1.call-start = ((), (), s32[]{:S(2)}) async-start(), calls=%async_computation.9 | async-start | bytes 1179648 | tf_op jit(solution)/shard_map/all_gather | solution.py:15
  126.3 79.4 %all-to-all-start.1 = ((bf16[16,8,2048]{2,0,1:T(8,128)(2,1)}), bf16[16,8,2048]{2,0,1:T(8,128)(2,1)}, u32[]{:S(2)}, u32[]{:S(2)}) async-start(bf16[16,8,2048]{2,0,1:T(8,128)(2,1)} %copy.134), calls=%async_computation.3 | async-start | bytes 1048576 | tf_op jit(solution)/shard_map/all_to_all | solution.py:241
  131.8 98.1 %all-gather.9.cloned.1.call-start = ((), (), s32[]{:S(2)}) async-start(), calls=%async_computation.7 | async-start | bytes 2621440 | tf_op jit(solution)/shard_map/all_gather | solution.py:242
  207.8 49.3 %reduce-scatter.3.cloned.1.call-start = ((), (), s32[]{:S(2)}) async-start(), calls=%async_computation.4 | async-start | bytes 1310720 | tf_op jit(solution)/shard_map/reduce_scatter | solution.py:201
  224.8 3.2 %copy-start.13 = (bf16[256,512]{1,0:T(8,128)(2,1)S(1)}, bf16[256,512]{1,0:T(8,128)(2,1)}, u32[]{:S(2)}) copy-start(bf16[256,512]{1,0:T(8,128)(2,1)} %param.26) | copy-start | bytes 786436
  227.9 1.8 copy-start.10
Sparse Core Ops, SparseCore 0:
  51.5 23.9 all-gather.6
  92.9 31.1 reduce-scatter.4
  207.9 21.2 all-gather.8
  232.2 24.8 reduce-scatter.2
Sparse Core Ops, SparseCore 1:
  109.4 45.0 all-gather.10
  156.4 38.6 all-gather.12
where the time goes:
time: 266 us; the launch traced here: 264 us
  waiting for transfers between devices  102 us (38%)
  matrix products  71.2 us (27%)
  local copies, waits for them, and re-layouts  35.6 us (13%)
  other arithmetic  25.2 us (9%)
  between operations  15.7 us (6%)
  starting transfers between devices  13.3 us (5%)
    all_gather x2, waiting for transfers between devices, carried_in(): lax.all_gather(part.astype(kind), axis)  63.2 us
    dot_general x54, matrix products, exact_product(): return jnp.matmul(left, right, precision=lax.Precision.HIGHEST)  52.1 us
    all_gather x1, waiting for transfers between devices, local(): piece = lax.all_gather(arrived, 'tp', axis=0, tiled=True)  14.3 us
    reduce_scatter x1, waiting for transfers between devices, local(): lax.psum_scatter(jnp.dot(normed, result_mapping_weights, preferred_elemen...  12.9 us
    reduce_scatter x1, waiting for transfers between devices, local(): lax.psum_scatter(jnp.dot(hidden, specialist_contract_weights[0], preferre...  11.9 us
    dot_general x1, matrix products, local(): jnp.dot(hidden, specialist_contract_weights[0], preferred_element_type=jn...  10.8 us
    all_to_all x1, starting transfers between devices, local(): lax.all_to_all(fill_slots(own_table, normed_in), 'ep', split_axis=1, conc...  7.41 us
    dot_general x1, matrix products, expert_hidden(): gate = jnp.dot(rows_in, gate_weight, preferred_element_type=jnp.float32)  6.48 us
  transfers between devices with their start and end apart: 8, of which 5 were waited for; matrix products, arithmetic and copies ran while one was open for 38% of the time, Pallas kernels for 0%

commit v1 on v0

v1 whole, which is shorter than its diff:
```python
import functools

import jax
import jax.numpy as jnp
from jax import lax
from jax.experimental import pallas as pl
from jax.experimental.pallas import tpu as pltpu
from jax.sharding import PartitionSpec as P

BLK = 64
EPS = 1e-06
F32 = jnp.float32
BF = jnp.bfloat16
LIMIT = 60 * 1024 * 1024


def call(body, outs, flops, name, scratch=()):
    return pl.pallas_call(
        body,
        out_shape=outs,
        scratch_shapes=list(scratch),
        name=name,
        cost_estimate=pl.CostEstimate(flops=flops, bytes_accessed=1 << 21, transcendentals=0),
        compiler_params=pltpu.CompilerParams(vmem_limit_bytes=LIMIT),
    )


def mm(a, b):
    return jnp.dot(a, b, preferred_element_type=F32)


def mm_nt(a, b):
    return lax.dot_general(a, b, (((1,), (1,)), ((), ())), preferred_element_type=F32)


def mm_tn(a, b, precision=None):
    return lax.dot_general(
        a, b, (((0,), (0,)), ((), ())), preferred_element_type=F32, precision=precision
    )


def unit(x):
    return x * lax.rsqrt(jnp.sum(x * x, axis=-1, keepdims=True) + EPS)


def span_kernel(heads, q_ref, k_ref, v_ref, w_ref, f_ref, x_ref, s_ref, off_ref, map_ref, loc_ref, eff_ref):
    rows = q_ref.shape[0]
    dk = q_ref.shape[1] // heads
    dv = v_ref.shape[1] // heads
    blocks = rows // BLK
    f = f_ref[...]
    soft = jnp.maximum(f, 0.0) + jnp.log(1.0 + jnp.exp(-jnp.abs(f)))
    g = x_ref[...] - s_ref[...] * soft
    write = 1.0 / (1.0 + jnp.exp(-w_ref[...]))
    ri = lax.broadcasted_iota(jnp.int32, (BLK, BLK), 0)
    ci = lax.broadcasted_iota(jnp.int32, (BLK, BLK), 1)
    inclusive = ri >= ci
    strict = ri > ci
    tril = inclusive.astype(F32)
    triu = (ri <= ci).astype(F32)
    eye = (ri == ci).astype(F32)
    masks = []
    size = 1
    while size < BLK:
        masks.append((ri // (2 * size) == ci // (2 * size)) & (ri // size != ci // size) & strict)
        size *= 2
    hi = lax.Precision.HIGHEST
    run_c, run_r = [], []
    for b in range(blocks):
        gb = g[b * BLK : (b + 1) * BLK]
        run_c.append(jnp.dot(tril, gb, preferred_element_type=F32, precision=hi))
        run_r.append(mm_tn(gb, triu, hi))
    lows, scores, rhs, qfs, kfs, ends = [], [], [], [], [], []
    for h in range(heads):
        for b in range(blocks):
            rs = slice(b * BLK, (b + 1) * BLK)
            q = unit(q_ref[rs, h * dk : (h + 1) * dk].astype(F32))
            k = unit(k_ref[rs, h * dk : (h + 1) * dk].astype(F32))
            v = v_ref[rs, h * dv : (h + 1) * dv].astype(F32)
            kb = k.astype(BF)
            rc = run_c[b][:, h : h + 1]
            rr = run_r[b][h : h + 1, :]
            wr = write[rs, h : h + 1]
            spread = rc - rr
            fade = jnp.where(inclusive, jnp.exp(jnp.where(inclusive, spread, 0.0)), 0.0)
            lows.append(jnp.where(strict, mm_nt(kb, kb) * fade * wr, 0.0))
            scores.append((mm_nt(q.astype(BF), kb) * fade).astype(BF))
            grown = jnp.exp(rc)
            last = rc[BLK - 1 : BLK, :]
            rhs.append(jnp.concatenate([v * wr, k * (wr * grown)], axis=1).astype(BF))
            qfs.append((q * grown).astype(BF))
            kfs.append((k * jnp.exp(last - rc)).astype(BF))
            ends.append(jnp.exp(last))
    count = heads * blocks
    inv = [eye - jnp.where(masks[0], lows[i], 0.0) for i in range(count)]
    for mask in masks[1:]:
        xb = [inv[i].astype(BF) for i in range(count)]
        mid = [mm(jnp.where(mask, lows[i], 0.0).astype(BF), xb[i]).astype(BF) for i in range(count)]
        inv = [inv[i] - mm(xb[i], mid[i]) for i in range(count)]
    both = [mm(inv[i].astype(BF), rhs[i]) for i in range(count)]
    dki = lax.broadcasted_iota(jnp.int32, (dk, dk), 0)
    dkj = lax.broadcasted_iota(jnp.int32, (dk, dk), 1)
    start = jnp.concatenate([jnp.zeros((dk, dv), F32), (dki == dkj).astype(F32)], axis=1)
    state = [start for _ in range(heads)]
    zero = jnp.zeros((BLK, dk), F32)
    for b in range(blocks):
        rs = slice(b * BLK, (b + 1) * BLK)
        at = [h * blocks + b for h in range(heads)]
        sb = [state[h].astype(BF) for h in range(heads)]
        fresh = [
            (
                jnp.concatenate([both[i][:, :dv], zero], axis=1)
                - mm(both[i][:, dv:].astype(BF), sb[h])
            ).astype(BF)
            for h, i in enumerate(at)
        ]
        for h, i in enumerate(at):
            reads = mm(qfs[i], sb[h]) + mm(scores[i], fresh[h])
            loc_ref[rs, h * dv : (h + 1) * dv] = reads[:, :dv]
            eff_ref[rs, h * dk : (h + 1) * dk] = reads[:, dv:].astype(BF)
        state = [state[h] * ends[i] + mm_tn(kfs[i], fresh[h]) for h, i in enumerate(at)]
    for h in range(heads):
        off_ref[h] = state[h][:, :dv].astype(BF)
        map_ref[h] = state[h][:, dv:].astype(BF)


def fold_kernel(in_ref, out_ref):
    length, dk, width = in_ref.shape
    cols = width - dk
    state = jnp.zeros((dk, cols), F32)
    for k in range(length):
        top = state.astype(BF)
        out_ref[k] = top
        if k + 1 < length:
            rest = (state - top.astype(F32)).astype(BF)
            step = in_ref[k, :, :dk]
            state = mm(step, top) + mm(step, rest) + in_ref[k, :, dk:].astype(F32)


def project_kernel(heads, loc_ref, eff_ref, state_ref, gate_ref, gain_ref, weight_ref, out_ref, normed):
    dv = loc_ref.shape[1] // heads
    dk = eff_ref.shape[1] // heads
    for h in range(heads):
        cs = slice(h * dv, (h + 1) * dv)
        reads = loc_ref[:, cs] + mm(eff_ref[:, h * dk : (h + 1) * dk], state_ref[h])
        scale = lax.rsqrt(jnp.mean(reads * reads, axis=-1, keepdims=True) + EPS)
        gate = gate_ref[:, cs].astype(F32)
        gate = gate / (1.0 + jnp.exp(-gate))
        normed[:, cs] = (reads * scale * gain_ref[...] * gate).astype(BF)
    step = min(512, out_ref.shape[1])
    for n in range(out_ref.shape[1] // step):
        ns = slice(n * step, (n + 1) * step)
        out_ref[:, ns] = mm(normed[...], weight_ref[:, ns]).astype(BF)


def slot_places(route, experts):
    tokens, picks = route.shape
    ids = lax.broadcasted_iota(jnp.int32, (tokens, experts), 1)
    chosen = [(route[:, j : j + 1] == ids).astype(F32) for j in range(picks)]
    total = functools.reduce(jnp.add, chosen)
    ti = lax.broadcasted_iota(jnp.int32, (tokens, tokens), 0)
    tj = lax.broadcasted_iota(jnp.int32, (tokens, tokens), 1)
    before = mm((ti > tj).astype(BF), total.astype(BF))
    return [jnp.sum(before * c, axis=1, keepdims=True).astype(jnp.int32) for c in chosen]


def dispatch_kernel(experts, share, x_ref, gain_ref, route_ref, out_ref):
    x = x_ref[...].astype(F32)
    normed = (
        x * lax.rsqrt(jnp.mean(x * x, axis=-1, keepdims=True) + EPS) * gain_ref[...]
    ).astype(BF)
    route = route_ref[...]
    tokens = route.shape[0]
    first = lax.axis_index("tp") * share
    slots = lax.broadcasted_iota(jnp.int32, (tokens, experts * share), 1)
    taken = jnp.zeros((tokens, experts * share), F32)
    for j, place in enumerate(slot_places(route, experts)):
        local = place - first
        target = jnp.where((local >= 0) & (local < share), route[:, j : j + 1] * share + local, -1)
        taken = taken + (slots == target).astype(F32)
    out_ref[...] = mm_tn(taken.astype(BF), normed).astype(BF)


def combine_kernel(experts, capacity, y_ref, route_ref, score_ref, out_ref):
    route = route_ref[...]
    tokens = route.shape[0]
    score = score_ref[...]
    score = score / jnp.sum(score, axis=1, keepdims=True)
    slots = lax.broadcasted_iota(jnp.int32, (tokens, experts * capacity), 1)
    total = jnp.zeros(out_ref.shape, F32)
    for j, place in enumerate(slot_places(route, experts)):
        target = route[:, j : j + 1] * capacity + place
        total = total + score[:, j : j + 1] * mm((slots == target).astype(BF), y_ref[...])
    out_ref[...] = total.astype(BF)


def expert_kernel(x_ref, g_ref, u_ref, d_ref, out_ref, acc):
    i = pl.program_id(0)
    groups, rows, cols = out_ref.shape
    gate = mm(x_ref[...], g_ref[0])
    up = mm(x_ref[...], u_ref[0])
    hidden = (gate / (1.0 + jnp.exp(-gate)) * up).astype(BF)

    @pl.when(i == 0)
    def _():
        for n in range(groups):
            acc[n] = mm(hidden, d_ref[0, :, n * cols : (n + 1) * cols])

    @pl.when(i > 0)
    def _():
        for n in range(groups):
            acc[n] += mm(hidden, d_ref[0, :, n * cols : (n + 1) * cols])

    @pl.when(i == pl.num_programs(0) - 1)
    def _():
        for n in range(groups):
            out_ref[n] = acc[n].astype(BF)


def experts_of(x, gate, up, down, groups):
    rows, width = x.shape
    ff = gate.shape[2]
    tile = min(256, ff)
    cols = width // groups
    return pl.pallas_call(
        expert_kernel,
        grid=(ff // tile,),
        in_specs=[
            pl.BlockSpec((rows, width), lambda i: (0, 0)),
            pl.BlockSpec((1, width, tile), lambda i: (0, 0, i)),
            pl.BlockSpec((1, width, tile), lambda i: (0, 0, i)),
            pl.BlockSpec((1, tile, width), lambda i: (0, i, 0)),
        ],
        out_specs=pl.BlockSpec((groups, rows, cols), lambda i: (0, 0, 0)),
        out_shape=jax.ShapeDtypeStruct((groups, rows, cols), BF),
        scratch_shapes=[pltpu.VMEM((groups, rows, cols), F32)],
        name="experts",
        cost_estimate=pl.CostEstimate(
            flops=6 * rows * width * ff, bytes_accessed=6 * width * ff, transcendentals=rows * ff
        ),
        compiler_params=pltpu.CompilerParams(vmem_limit_bytes=LIMIT),
    )(x, gate, up, down)


def swap(value, bit, size):
    return lax.ppermute(value, "tp", [(j, j ^ bit) for j in range(size)])


def scatter_sum(parts, size):
    mine = lax.axis_index("tp")
    bit = 1
    rest = parts
    while bit < size:
        pairs = rest.reshape((rest.shape[0] // 2, 2) + rest.shape[1:])
        upper = (mine // bit) % 2
        keep = lax.dynamic_index_in_dim(pairs, upper, 1, keepdims=False)
        give = lax.dynamic_index_in_dim(pairs, 1 - upper, 1, keepdims=False)
        got = swap(give, bit, size)
        rest = (keep.astype(F32) + got.astype(F32)).astype(BF)
        bit *= 2
    return rest[0]


def gather_all(value, size):
    mine = lax.axis_index("tp")
    bit = size // 2
    rest = value[None]
    while bit >= 1:
        got = swap(rest, bit, size)
        upper = (mine // bit) % 2 == 1
        low = jnp.where(upper, got, rest)
        high = jnp.where(upper, rest, got)
        rest = jnp.stack([low, high], axis=1).reshape((2 * rest.shape[0],) + value.shape)
        bit //= 2
    return rest


def local(
    initial_micro_probes,
    initial_micro_lookup_keys,
    initial_micro_payloads,
    result_switch_preactivation,
    insertion_power_preactivation,
    fading_preactivation,
    extra_fading_term,
    channel_fading_speed,
    result_scaling_vector,
    result_mapping_weights,
    latter_micro_entries,
    specialist_scaling_vector,
    selected_specialists,
    selected_dispatch_weights,
    specialist_switch_weights,
    specialist_expand_weights,
    specialist_contract_weights,
):
    groups = lax.axis_size("tp")
    length = lax.axis_size("ep")
    rows = initial_micro_probes.shape[0]
    heads = channel_fading_speed.shape[0]
    dk = initial_micro_probes.shape[1] // heads
    dv = initial_micro_payloads.shape[1] // heads
    tokens, width = latter_micro_entries.shape
    picks = selected_specialists.shape[1]
    experts = length
    capacity = 2 * tokens * picks // experts
    share = capacity // groups
    shape = jax.ShapeDtypeStruct

    sent = call(
        functools.partial(dispatch_kernel, experts, share),
        shape((experts * share, width), BF),
        2 * tokens * experts * share * width,
        "dispatch",
    )(latter_micro_entries, specialist_scaling_vector[None], selected_specialists)
    arrived = lax.all_to_all(
        sent.reshape(experts, share, width), "ep", split_axis=0, concat_axis=0, tiled=True
    )

    offset, mapping, located, effect = call(
        functools.partial(span_kernel, heads),
        (
            shape((heads, dk, dv), BF),
            shape((heads, dk, dk), BF),
            shape((rows, heads * dv), F32),
            shape((rows, heads * dk), BF),
        ),
        12 * 10**9,
        "spans",
    )(
        initial_micro_probes,
        initial_micro_lookup_keys,
        initial_micro_payloads,
        insertion_power_preactivation,
        fading_preactivation,
        extra_fading_term,
        channel_fading_speed[None],
    )

    pieces = gather_all(arrived.reshape(experts * share, width), groups)
    partial_sums = experts_of(
        pieces.reshape(groups * experts * share, width),
        specialist_switch_weights,
        specialist_expand_weights,
        specialist_contract_weights,
        groups,
    )

    slices = length // heads
    cols = dv // slices
    cut = jnp.transpose(offset.reshape(heads, dk, slices, cols), (0, 2, 1, 3)).reshape(
        length, dk, cols
    )
    copied = jnp.broadcast_to(mapping[:, None], (heads, slices, dk, dk)).reshape(length, dk, dk)
    spans = lax.all_to_all(
        jnp.concatenate([copied, cut], axis=2), "ep", split_axis=0, concat_axis=0, tiled=True
    )
    befores = call(
        fold_kernel, shape((length, dk, cols), BF), length * 4 * dk * dk * cols, "fold"
    )(spans)
    prior = lax.all_to_all(befores, "ep", split_axis=0, concat_axis=0, tiled=True)
    prior = jnp.transpose(prior.reshape(heads, slices, dk, cols), (0, 2, 1, 3)).reshape(
        heads, dk, dv
    )
    projected = call(
        functools.partial(project_kernel, heads),
        shape((rows, result_mapping_weights.shape[1]), BF),
        2 * rows * heads * dv * result_mapping_weights.shape[1],
        "project",
        [pltpu.VMEM((rows, heads * dv), BF)],
    )(
        located,
        effect,
        prior,
        result_switch_preactivation,
        result_scaling_vector[None],
        result_mapping_weights,
    )
    mixer_out = scatter_sum(projected.reshape(groups, rows // groups, -1), groups)

    summed = scatter_sum(partial_sums, groups)
    summed = summed.reshape(groups, experts, share, width // groups)
    summed = jnp.transpose(summed, (1, 0, 2, 3)).reshape(experts, capacity, width // groups)
    returned = lax.all_to_all(summed, "ep", split_axis=0, concat_axis=0, tiled=True)
    combined = call(
        functools.partial(combine_kernel, experts, capacity),
        shape((tokens, width // groups), BF),
        4 * tokens * experts * capacity * (width // groups),
        "combine",
    )(
        returned.reshape(experts * capacity, width // groups),
        selected_specialists,
        selected_dispatch_weights,
    )
    moe_out = jnp.transpose(gather_all(combined, groups), (1, 0, 2)).reshape(tokens, width)
    return (mixer_out, moe_out)


def solution(mesh):
    return jax.shard_map(
        local,
        mesh=mesh,
        in_specs=(
            P("ep", "tp"),
            P("ep", "tp"),
            P("ep", "tp"),
            P("ep", "tp"),
            P("ep", "tp"),
            P("ep", "tp"),
            P("ep", "tp"),
            P("tp"),
            P(),
            P("tp", None),
            P("ep", None),
            P(),
            P("ep", None),
            P("ep", None),
            P("ep", None, "tp"),
            P("ep", None, "tp"),
            P("ep", "tp", None),
        ),
        out_specs=(P(("ep", "tp"), None), P("ep", None)),
        check_vma=False,
    )
```

time: 266 us -> 145 us (0.55)
  matrix products: 71.2 us -> 0 us
  waiting for transfers between devices: 102 us -> 49.3 us
  Pallas kernels: 0 us -> 30.5 us
  blocking collectives: 0 us -> 21.8 us
  local copies, waits for them, and re-layouts: 35.6 us -> 17.5 us
  other arithmetic: 25.2 us -> 7.24 us
  between operations: 15.7 us -> 0.79 us
  starting transfers between devices: 13.3 us -> 16.9 us
    all_gather x4 -> x0, waiting for transfers between devices: 77.5 us -> none  [the longest x2 63.2 us: carried_in(): lax.all_gather(part.astype(kind), axis)]
    dot_general x57 -> x0, matrix products: 71.2 us -> none  [the longest x54 52.1 us: exact_product(): return jnp.matmul(left, right, precision=lax.Precision.HIGHEST)]
    pallas_call x0 -> x6, Pallas kernels: none -> 30.5 us  [the longest x1 12.5 us: experts_of(): pl.pallas_call(expert_kernel, grid=(ff // tile,), in_specs=[pl.BlockSpec(...]
    all_to_all x2 -> x3, waiting for transfers between devices: 0.01 us -> 30.1 us  [the longest x1 14.5 us: local(): lax.all_to_all(summed, 'ep', split_axis=0, concat_axis=0, tiled=True)]
    reduce_scatter x2 -> x0, waiting for transfers between devices: 24.8 us -> none  [the longest x1 12.9 us: local(): lax.psum_scatter(jnp.dot(normed, result_mapping_weights, preferred_elemen...]
    all_to_all x0 -> x1, blocking collectives: none -> 21.8 us  [local(): lax.all_to_all(sent.reshape(experts, share, width), 'ep', split_axis=0, c...]
    ppermute x0 -> x8, waiting for transfers between devices: none -> 19.2 us  [swap(): return lax.ppermute(value, 'tp', [(j, j ^ bit) for j in range(size)])]
    reduce_sum x7 -> x0, other arithmetic: 11.2 us -> none  [the longest x1 5.74 us: local(): jnp.sum(values.astype(jnp.float32) * route_weight[..., None], axis=1)]
  transfers between devices with their start and end apart: 8 -> 11, of which waited for: 5 -> 7; matrix products, arithmetic and copies ran while one was open for 38% -> 12% of each run, Pallas kernels for 0% -> 9%
where the time goes in v1:
time: 145 us; the launch traced here: 144 us
  waiting for transfers between devices  49.3 us (34%)
  Pallas kernels  30.5 us (21%)
  blocking collectives  21.8 us (15%)
  local copies, waits for them, and re-layouts  17.5 us (12%)
  starting transfers between devices  16.9 us (12%)
  other arithmetic  7.24 us (5%)
    all_to_all x1, blocking collectives, local(): lax.all_to_all(sent.reshape(experts, share, width), 'ep', split_axis=0, c...  21.8 us
    ppermute x8, waiting for transfers between devices, swap(): return lax.ppermute(value, 'tp', [(j, j ^ bit) for j in range(size)])  19.2 us
    all_to_all x1, waiting for transfers between devices, local(): lax.all_to_all(summed, 'ep', split_axis=0, concat_axis=0, tiled=True)  14.5 us
    pallas_call x1, Pallas kernels, experts_of(): pl.pallas_call(expert_kernel, grid=(ff // tile,), in_specs=[pl.BlockSpec(...  12.5 us
    all_to_all x1, waiting for transfers between devices, local(): lax.all_to_all(jnp.concatenate([copied, cut], axis=2), 'ep', split_axis=0...  8.3 us
    all_to_all x1, waiting for transfers between devices, local(): lax.all_to_all(befores, 'ep', split_axis=0, concat_axis=0, tiled=True)  7.34 us
    unnamed x20, local copies, waits for them, and re-layouts  6.39 us
    pallas_call x1, Pallas kernels, local(): call(functools.partial(span_kernel, heads), (shape((heads, dk, dv), BF),...  6 us
  transfers between devices with their start and end apart: 11, of which 7 were waited for; matrix products, arithmetic and copies ran while one was open for 12% of the time, Pallas kernels for 9%

profile of v1, /device:TPU:0, one launch (start us, length us, event | category | flops | bytes accessed | tf_op | source)
XLA Modules:
  0.0 144.1 jit_solution(3574207197596452781)
XLA Ops:
  0.6 1.4 copy.64.route_ref
  2.0 2.6 %dispatch.1 = bf16[128,2048]{1,0:T(8,128)(2,1)} custom-call(bf16[128,2048]{1,0:T(8,128)(2,1)} %x_ref.2, f32[1,2048]{1,0:T(1,128)} %bitcast.90, s32[128,2]{1,0:T(8,128)} %copy.64.route_ref), custom_call_target="tpu_custom_call" | custom-call | flops 67108864 | bytes 2097152 | tf_op jit(solution)/shard_map/dispatch/pallas_call | solution.py:310
  4.7 21.8 %all_to_all.20 = bf16[8,16,2048]{2,1,0:T(8,128)(2,1)S(1)} all-to-all(bf16[8,16,2048]{2,1,0:T(8,128)(2,1)} %bitcast.85), channel_id=1, replica_groups=mesh['ep'=8,'tp'=4] {'ep'}, dimensions={0} | all-to-all | bytes 1048576 | tf_op jit(solution)/shard_map/all_to_all | solution.py:316
  26.5 1.5 %collective-permute-start.2 = (bf16[1,128,2048]{2,1,0:T(8,128)(2,1)S(1)}, bf16[1,128,2048]{2,1,0:T(8,128)(2,1)S(1)}, u32[]{:S(2)}, u32[]{:S(2)}) collective-permute-start(bf16[1,128,2048]{2,1,0:T(8,128)(2,1)S(1)} %bitcast.76), channel_id=1, source_target_pairs={{0,2},{1,3},{2,0},{3,1},{4,6},{5,7},{6,4},{7,5},{8,10},{9,11},{10,... | collective-permute-start | bytes 1572872 | tf_op jit(solution)/shard_map/ppermute | solution.py:246
  28.0 11.0 %collective-permute-done.2 = bf16[1,128,2048]{2,1,0:T(8,128)(2,1)S(1)} collective-permute-done((bf16[1,128,2048]{2,1,0:T(8,128)(2,1)S(1)}, bf16[1,128,2048]{2,1,0:T(8,128)(2,1)S(1)}, u32[]{:S(2)}, u32[]{:S(2)}) %collective-permute-start.2) | collective-permute-done | bytes 524320 | tf_op jit(solution)/shard_map/ppermute | solution.py:246
  39.0 0.1 select_bitcast_fusion.3
  39.1 1.1 maximum_bitcast_fusion
  40.2 0.0 collective-permute-start.3
  40.2 0.0 copy-done.3
  40.2 0.8 copy.55.w_ref
  41.0 0.0 copy-done.4
  41.0 0.8 copy.56.f_ref
  41.8 0.0 copy-done.5
  41.8 0.8 copy.57.x_ref
  42.6 0.5 collective-permute-done.3
  43.1 0.1 select_bitcast_fusion.1
  43.2 1.5 %pad_maximum_fusion = bf16[2,2,128,2048]{3,2,1,0:T(8,128)(2,1)} fusion(bf16[2,1,128,2048]{3,2,1,0:T(8,128)(2,1)S(1)} %get-tuple-element.15, bf16[2,1,128,2048]{3,2,1,0:T(8,128)(2,1)S(1)} %get-tuple-element.14), kind=kLoop, calls=%fused_computation | loop fusion | flops 1048576 | bytes 4194304 | tf_op jit(solution)/shard_map/stack | solution.py:273
  44.7 12.5 %experts.1 = bf16[4,512,512]{2,1,0:T(8,128)(2,1)} custom-call(bf16[512,2048]{1,0:T(8,128)(2,1)} %bitcast.80, bf16[1,2048,1024]{2,1,0:T(8,128)(2,1)} %g_ref.1, bf16[1,2048,1024]{2,1,0:T(8,128)(2,1)} %u_ref.1, bf16[1,1024,2048]{2,1,0:T(8,128)(2,1)} %d_ref.1), custom_call_target="tpu_custom_call" | custom-call | flops 6442450944 | bytes 12582912 | tf_op jit(solution)/shard_map/experts/pallas_call | solution.py:225
  57.2 1.3 dynamic-slice_bitcast_fusion
  58.5 0.2 collective-permute-start.4
  58.7 6.0 %spans.1 = (bf16[4,128,128]{2,1,0:T(8,128)(2,1)}, bf16[4,128,128]{2,1,0:T(8,128)(2,1)}, f32[256,512]{1,0:T(8,128)}, bf16[256,512]{1,0:T(8,128)(2,1)}) custom-call(bf16[256,512]{1,0:T(8,128)(2,1)} %q_ref.1, bf16[256,512]{1,0:T(8,128)(2,1)} %k_ref.1, bf16[256,512]{1,0:T(8,128)(2,1)} %v_ref.1, f32[256,4]{1,0:T(8,128)} %copy.55.w_ref, f32[256,4]{1,0:T(8,128)} %copy.56.f_ref, ...), custom_call_target="tpu_custom_call" | custom-call | flops 12000000000 | bytes 2097152 | tf_op jit(solution)/shard_map/spans/pallas_call | solution.py:320
  64.7 1.2 fusion.3
  65.9 0.1 pad_maximum_fusion.3
  66.0 0.1 copy.59
  66.2 1.0 copy.58
  67.2 0.8 pad_maximum_fusion.2
  68.0 4.4 %all-to-all-start = ((bf16[8,128,192]{1,2,0:T(8,128)(2,1)}), bf16[8,128,192]{1,2,0:T(8,128)(2,1)S(1)}, u32[]{:S(2)}, u32[]{:S(2)}) async-start(bf16[8,128,192]{1,2,0:T(8,128)(2,1)} %pad_maximum_fusion.2), calls=%async_computation | async-start | bytes 786432 | tf_op jit(solution)/shard_map/all_to_all | solution.py:355
  72.4 0.0 collective-permute-done.4
  72.4 1.5 %fusion = bf16[2,512,512]{2,1,0:T(8,128)(2,1)S(1)} fusion(bf16[2,512,512]{2,1,0:T(8,128)(2,1)} %collective-permute-done.4, bf16[2,2,512,512]{3,2,1,0:T(8,128)(2,1)S(1)} %bitcast.79, s32[]{:T(128)S(6)} %select_n.103), kind=kLoop, calls=%fused_computation.2 | loop fusion | flops 2097152 | bytes 3145732 | tf_op jit(solution)/shard_map/convert_element_type | solution.py:259
  73.9 0.9 constant_dynamic-slice_fusion
  74.8 1.5 %collective-permute-start.5 = (bf16[1,512,512]{2,1,0:T(8,128)(2,1)}, bf16[1,512,512]{2,1,0:T(8,128)(2,1)S(1)}, u32[]{:S(2)}, u32[]{:S(2)}) collective-permute-start(bf16[1,512,512]{2,1,0:T(8,128)(2,1)} %constant_dynamic-slice_fusion), channel_id=1, source_target_pairs={{0,2},{1,3},{2,0},{3,1},{4,6},{5,7},{6,4},{7,5},{8,10},{9,11},{10,... | collective-permute-start | bytes 1572872 | tf_op jit(solution)/shard_map/ppermute | solution.py:246
  76.3 8.3 %all-to-all-done = bf16[8,128,192]{1,2,0:T(8,128)(2,1)S(1)} async-done(((bf16[8,128,192]{1,2,0:T(8,128)(2,1)}), bf16[8,128,192]{1,2,0:T(8,128)(2,1)S(1)}, u32[]{:S(2)}, u32[]{:S(2)}) %all-to-all-start) | async-done | bytes 393248 | tf_op jit(solution)/shard_map/all_to_all | solution.py:355
  84.6 1.0 copy.60.in_ref
  85.6 2.8 %fold.1 = bf16[8,128,64]{2,1,0:T(8,128)(2,1)} custom-call(bf16[8,128,192]{2,1,0:T(8,128)(2,1)} %copy.60.in_ref), custom_call_target="tpu_custom_call" | custom-call | flops 33554432 | bytes 2097152 | tf_op jit(solution)/shard_map/fold/pallas_call | solution.py:358
  88.4 1.7 %copy.61 = bf16[8,128,64]{1,2,0:T(8,128)(2,1)} copy(bf16[8,128,64]{2,1,0:T(8,128)(2,1)} %fold.1) | data formatting | bytes 262144 | tf_op jit(solution)/shard_map/fold/pallas_call | solution.py:358
  90.1 3.6 %all-to-all-start.1 = ((bf16[8,128,64]{1,2,0:T(8,128)(2,1)}), bf16[8,128,64]{1,2,0:T(8,128)(2,1)S(1)}, u32[]{:S(2)}, u32[]{:S(2)}) async-start(bf16[8,128,64]{1,2,0:T(8,128)(2,1)} %copy.61), calls=%async_computation.1 | async-start | bytes 262144 | tf_op jit(solution)/shard_map/all_to_all | solution.py:361
  93.8 7.3 %all-to-all-done.1 = bf16[8,128,64]{1,2,0:T(8,128)(2,1)S(1)} async-done(((bf16[8,128,64]{1,2,0:T(8,128)(2,1)}), bf16[8,128,64]{1,2,0:T(8,128)(2,1)S(1)}, u32[]{:S(2)}, u32[]{:S(2)}) %all-to-all-start.1) | async-done | bytes 131104 | tf_op jit(solution)/shard_map/all_to_all | solution.py:361
  101.1 0.8 copy.62.state_ref
  101.9 4.1 %project.1 = bf16[256,2048]{1,0:T(8,128)(2,1)} custom-call(f32[256,512]{1,0:T(8,128)} %get-tuple-element.6.loc_ref, bf16[256,512]{1,0:T(8,128)(2,1)} %get-tuple-element.7.eff_ref, bf16[4,128,128]{2,1,0:T(8,128)(2,1)} %copy.62.state_ref, bf16[256,512]{1,0:T(8,128)(2,1)} %gate_ref.1, f32[1,128]{1,0:T(1,128)} %bitcast.91, bf16[512,2048]{1,0:T(8,128)(2,1)} %weight_ref.1), custom_call_target="tpu_custom_call" | custom-call | flops 536870912 | bytes 2097152 | tf_op jit(solution)/shard_map/project/pallas_call | solution.py:365
  105.9 1.9 %dynamic-slice_bitcast_fusion.1 = bf16[2,64,2048]{2,1,0:T(8,128)(2,1)} fusion(bf16[2,2,64,2048]{3,2,1,0:T(8,128)(2,1)} %bitcast.74, s32[]{:T(128)S(6)} %select_n.104), kind=kLoop, calls=%fused_computation.14 | loop fusion | bytes 1048580 | tf_op jit(solution)/shard_map/jit(dynamic_index_in_dim)/squeeze | solution.py:257
  107.8 0.0 collective-permute-start
  107.8 0.0 collective-permute-done.5
  107.8 0.1 add_convert_fusion
  108.0 0.9 copy.66
  108.8 3.5 %all-to-all-start.3 = ((bf16[8,64,512]{2,1,0:T(8,128)(2,1)}), bf16[8,64,512]{2,1,0:T(8,128)(2,1)S(1)}, u32[]{:S(2)}, u32[]{:S(2)}) async-start(bf16[8,64,512]{2,1,0:T(8,128)(2,1)} %bitcast.26), calls=%async_computation.3 | async-start | bytes 1048576 | tf_op jit(solution)/shard_map/all_to_all | solution.py:384
  112.3 0.0 copy-done.6
  112.4 0.7 copy.68.score_ref
  113.1 0.0 collective-permute-done
  113.1 0.0 copy-done
  113.1 0.1 fusion.1
  113.2 14.5 %all-to-all-done.3 = bf16[8,64,512]{2,1,0:T(8,128)(2,1)S(1)} async-done(((bf16[8,64,512]{2,1,0:T(8,128)(2,1)}), bf16[8,64,512]{2,1,0:T(8,128)(2,1)S(1)}, u32[]{:S(2)}, u32[]{:S(2)}) %all-to-all-start.3) | async-done | bytes 524320 | tf_op jit(solution)/shard_map/all_to_all | solution.py:384
  127.7 0.8 copy-done.2
  128.5 2.5 %combine.1 = bf16[128,512]{1,0:T(8,128)(2,1)} custom-call(bf16[512,512]{1,0:T(8,128)(2,1)} %bitcast.81, s32[128,2]{1,0:T(8,128)} %copy.64.route_ref, f32[128,2]{1,0:T(8,128)} %copy.68.score_ref), custom_call_target="tpu_custom_call" | custom-call | flops 134217728 | bytes 2097152 | tf_op jit(solution)/shard_map/combine/pallas_call | solution.py:385
  131.0 1.5 %collective-permute-start.6 = (bf16[1,128,512]{2,1,0:T(8,128)(2,1)}, bf16[1,128,512]{2,1,0:T(8,128)(2,1)S(1)}, u32[]{:S(2)}, u32[]{:S(2)}) collective-permute-start(bf16[1,128,512]{2,1,0:T(8,128)(2,1)} %bitcast.88), channel_id=1, source_target_pairs={{0,2},{1,3},{2,0},{3,1},{4,6},{5,7},{6,4},{7,5},{8,10},{9,11},{10,... | collective-permute-start | bytes 393224 | tf_op jit(solution)/shard_map/ppermute | solution.py:246
  132.5 0.6 collective-permute-start.1
  133.1 4.5 %collective-permute-done.6 = bf16[1,128,512]{2,1,0:T(8,128)(2,1)S(1)} collective-permute-done((bf16[1,128,512]{2,1,0:T(8,128)(2,1)}, bf16[1,128,512]{2,1,0:T(8,128)(2,1)S(1)}, u32[]{:S(2)}, u32[]{:S(2)}) %collective-permute-start.6) | collective-permute-done | bytes 131104 | tf_op jit(solution)/shard_map/ppermute | solution.py:246
  137.6 0.9 select_bitcast_fusion.7
  138.5 0.1 collective-permute-start.7
  138.6 3.2 %collective-permute-done.1 = bf16[1,64,2048]{2,1,0:T(8,128)(2,1)S(1)} collective-permute-done((bf16[1,64,2048]{2,1,0:T(8,128)(2,1)S(1)}, bf16[1,64,2048]{2,1,0:T(8,128)(2,1)S(1)}, u32[]{:S(2)}, u32[]{:S(2)}) %collective-permute-start.1) | collective-permute-done | bytes 262176 | tf_op jit(solution)/shard_map/ppermute | solution.py:246
  141.9 0.8 fusion.2
  142.6 0.0 collective-permute-done.7
  142.7 0.1 pad_maximum_fusion.1
  142.8 0.3 copy.70
  143.0 1.0 copy.71
  (13 shorter events, 0.2 us)
Async XLA Ops:
  26.5 12.5 %collective-permute-start.2 = (bf16[1,128,2048]{2,1,0:T(8,128)(2,1)S(1)}, bf16[1,128,2048]{2,1,0:T(8,128)(2,1)S(1)}, u32[]{:S(2)}, u32[]{:S(2)}) collective-permute-start(bf16[1,128,2048]{2,1,0:T(8,128)(2,1)S(1)} %bitcast.76), channel_id=1, source_target_pairs={{0,2},{1,3},{2,0},{3,1},{4,6},{5,7},{6,4},{7,5},{8,10},{9,11},{10,... | collective-permute-start | bytes 1572872 | tf_op jit(solution)/shard_map/ppermute | solution.py:246
  39.0 1.2 copy-start.3
  39.0 2.0 %copy-start.4 = (f32[256,4]{0,1:T(4,128)S(1)}, f32[256,4]{0,1:T(4,128)}, u32[]{:S(2)}) copy-start(f32[256,4]{0,1:T(4,128)} %param.22) | copy-start | bytes 12292
  39.0 2.8 %copy-start.5 = (f32[256,4]{0,1:T(4,128)S(1)}, f32[256,4]{0,1:T(4,128)}, u32[]{:S(2)}) copy-start(f32[256,4]{0,1:T(4,128)} %param.23) | copy-start | bytes 12292
  40.2 2.9 %collective-permute-start.3 = (bf16[2,128,2048]{2,1,0:T(8,128)(2,1)}, bf16[2,128,2048]{2,1,0:T(8,128)(2,1)S(1)}, u32[]{:S(2)}, u32[]{:S(2)}) collective-permute-start(bf16[2,128,2048]{2,1,0:T(8,128)(2,1)} %maximum_bitcast_fusion), channel_id=1, source_target_pairs={{0,1},{1,0},{2,3},{3,2},{4,5},{5,4},{6,7},{7,6},{8,9},{9,8},{10,11... | collective-permute-start | bytes 3145736 | tf_op jit(solution)/shard_map/ppermute | solution.py:246
  58.5 13.9 %collective-permute-start.4 = (bf16[2,512,512]{2,1,0:T(8,128)(2,1)S(1)}, bf16[2,512,512]{2,1,0:T(8,128)(2,1)}, u32[]{:S(2)}, u32[]{:S(2)}) collective-permute-start(bf16[2,512,512]{2,1,0:T(8,128)(2,1)S(1)} %dynamic-slice_bitcast_fusion), channel_id=1, source_target_pairs={{0,1},{1,0},{2,3},{3,2},{4,5},{5,4},{6,7},{7,6},{8,9},{9,8},{10,11... | collective-permute-start | bytes 3145736 | tf_op jit(solution)/shard_map/ppermute | solution.py:246
  64.7 7.7 %copy-start.1 = (bf16[4,512,512]{2,1,0:T(8,128)(2,1)S(1)}, bf16[4,512,512]{2,1,0:T(8,128)(2,1)}, u32[]{:S(2)}) copy-start(bf16[4,512,512]{2,1,0:T(8,128)(2,1)} %experts.1) | copy-start | bytes 6291460
  68.0 16.6 %all-to-all-start = ((bf16[8,128,192]{1,2,0:T(8,128)(2,1)}), bf16[8,128,192]{1,2,0:T(8,128)(2,1)S(1)}, u32[]{:S(2)}, u32[]{:S(2)}) async-start(bf16[8,128,192]{1,2,0:T(8,128)(2,1)} %pad_maximum_fusion.2), calls=%async_computation | async-start | bytes 786432 | tf_op jit(solution)/shard_map/all_to_all | solution.py:355
  74.8 33.1 %collective-permute-start.5 = (bf16[1,512,512]{2,1,0:T(8,128)(2,1)}, bf16[1,512,512]{2,1,0:T(8,128)(2,1)S(1)}, u32[]{:S(2)}, u32[]{:S(2)}) collective-permute-start(bf16[1,512,512]{2,1,0:T(8,128)(2,1)} %constant_dynamic-slice_fusion), channel_id=1, source_target_pairs={{0,2},{1,3},{2,0},{3,1},{4,6},{5,7},{6,4},{7,5},{8,10},{9,11},{10,... | collective-permute-start | bytes 1572872 | tf_op jit(solution)/shard_map/ppermute | solution.py:246
  90.1 11.0 %all-to-all-start.1 = ((bf16[8,128,64]{1,2,0:T(8,128)(2,1)}), bf16[8,128,64]{1,2,0:T(8,128)(2,1)S(1)}, u32[]{:S(2)}, u32[]{:S(2)}) async-start(bf16[8,128,64]{1,2,0:T(8,128)(2,1)} %copy.61), calls=%async_computation.1 | async-start | bytes 262144 | tf_op jit(solution)/shard_map/all_to_all | solution.py:361
  107.8 4.5 %copy-start.6 = (f32[128,2]{0,1:T(2,128)S(1)}, f32[128,2]{0,1:T(2,128)}, u32[]{:S(2)}) copy-start(f32[128,2]{0,1:T(2,128)} %param.30) | copy-start | bytes 3076
  107.8 5.3 %copy-start = (bf16[256,2048]{1,0:T(8,128)(2,1)S(1)}, bf16[256,2048]{1,0:T(8,128)(2,1)}, u32[]{:S(2)}) copy-start(bf16[256,2048]{1,0:T(8,128)(2,1)} %project.1) | copy-start | bytes 3145732
  107.8 5.3 %collective-permute-start = (bf16[2,64,2048]{2,1,0:T(8,128)(2,1)}, bf16[2,64,2048]{2,1,0:T(8,128)(2,1)S(1)}, u32[]{:S(2)}, u32[]{:S(2)}) collective-permute-start(bf16[2,64,2048]{2,1,0:T(8,128)(2,1)} %dynamic-slice_bitcast_fusion.1), channel_id=1, source_target_pairs={{0,1},{1,0},{2,3},{3,2},{4,5},{5,4},{6,7},{7,6},{8,9},{9,8},{10,11... | collective-permute-start | bytes 1572872 | tf_op jit(solution)/shard_map/ppermute | solution.py:246
  108.8 18.9 %all-to-all-start.3 = ((bf16[8,64,512]{2,1,0:T(8,128)(2,1)}), bf16[8,64,512]{2,1,0:T(8,128)(2,1)S(1)}, u32[]{:S(2)}, u32[]{:S(2)}) async-start(bf16[8,64,512]{2,1,0:T(8,128)(2,1)} %bitcast.26), calls=%async_computation.3 | async-start | bytes 1048576 | tf_op jit(solution)/shard_map/all_to_all | solution.py:384
  127.7 0.8 copy-start.2
  131.0 6.6 %collective-permute-start.6 = (bf16[1,128,512]{2,1,0:T(8,128)(2,1)}, bf16[1,128,512]{2,1,0:T(8,128)(2,1)S(1)}, u32[]{:S(2)}, u32[]{:S(2)}) collective-permute-start(bf16[1,128,512]{2,1,0:T(8,128)(2,1)} %bitcast.88), channel_id=1, source_target_pairs={{0,2},{1,3},{2,0},{3,1},{4,6},{5,7},{6,4},{7,5},{8,10},{9,11},{10,... | collective-permute-start | bytes 393224 | tf_op jit(solution)/shard_map/ppermute | solution.py:246
  132.5 9.3 %collective-permute-start.1 = (bf16[1,64,2048]{2,1,0:T(8,128)(2,1)S(1)}, bf16[1,64,2048]{2,1,0:T(8,128)(2,1)S(1)}, u32[]{:S(2)}, u32[]{:S(2)}) collective-permute-start(bf16[1,64,2048]{2,1,0:T(8,128)(2,1)S(1)} %constant_dynamic-slice_fusion.1), channel_id=1, source_target_pairs={{0,2},{1,3},{2,0},{3,1},{4,6},{5,7},{6,4},{7,5},{8,10},{9,11},{10,... | collective-permute-start | bytes 786440 | tf_op jit(solution)/shard_map/ppermute | solution.py:246
  138.5 4.1 %collective-permute-start.7 = (bf16[2,128,512]{2,1,0:T(8,128)(2,1)S(1)}, bf16[2,128,512]{2,1,0:T(8,128)(2,1)S(1)}, u32[]{:S(2)}, u32[]{:S(2)}) collective-permute-start(bf16[2,128,512]{2,1,0:T(8,128)(2,1)S(1)} %maximum_bitcast_fusion.1), channel_id=1, source_target_pairs={{0,1},{1,0},{2,3},{3,2},{4,5},{5,4},{6,7},{7,6},{8,9},{9,8},{10,11... | collective-permute-start | bytes 786440 | tf_op jit(solution)/shard_map/ppermute | solution.py:246

commit v2 on v1

--- a/solution.py
+++ b/solution.py
@@ -43,7 +43,7 @@
     return x * lax.rsqrt(jnp.sum(x * x, axis=-1, keepdims=True) + EPS)
 
 
-def span_kernel(heads, q_ref, k_ref, v_ref, w_ref, f_ref, x_ref, s_ref, off_ref, map_ref, loc_ref, eff_ref):
+def span_kernel(heads, q_ref, k_ref, v_ref, w_ref, f_ref, x_ref, s_ref, pay_ref, loc_ref, eff_ref):
     rows = q_ref.shape[0]
     dk = q_ref.shape[1] // heads
     dv = v_ref.shape[1] // heads
@@ -120,21 +120,148 @@
             eff_ref[rs, h * dk : (h + 1) * dk] = reads[:, dv:].astype(BF)
         state = [state[h] * ends[i] + mm_tn(kfs[i], fresh[h]) for h, i in enumerate(at)]
     for h in range(heads):
-        off_ref[h] = state[h][:, :dv].astype(BF)
-        map_ref[h] = state[h][:, dv:].astype(BF)
+        pay_ref[h] = state[h].astype(BF)
 
 
 def fold_kernel(in_ref, out_ref):
     length, dk, width = in_ref.shape
-    cols = width - dk
-    state = jnp.zeros((dk, cols), F32)
+    state = jnp.zeros((dk, width - dk), F32)
     for k in range(length):
         top = state.astype(BF)
         out_ref[k] = top
         if k + 1 < length:
             rest = (state - top.astype(F32)).astype(BF)
-            step = in_ref[k, :, :dk]
-            state = mm(step, top) + mm(step, rest) + in_ref[k, :, dk:].astype(F32)
+            step = in_ref[k, :, width - dk :]
+            state = mm(step, top) + mm(step, rest) + in_ref[k, :, : width - dk].astype(F32)
+
+
+def flipped(index, bit):
+    return index + bit - 2 * bit * ((index // bit) % 2)
+
+
+def remote(src, dst, send, recv, where):
+    return pltpu.make_async_remote_copy(
+        src_ref=src,
+        dst_ref=dst,
+        send_sem=send,
+        recv_sem=recv,
+        device_id=where,
+        device_id_type=pl.DeviceIdType.MESH,
+    )
+
+
+def mix_kernel(
+    heads, length, groups,
+    sent_ref, q_ref, k_ref, v_ref, w_ref, f_ref, x_ref, s_ref,
+    out_ref, prior_ref, loc_ref, eff_ref,
+    held, pay, came, states, prior,
+    d_send, d_recv, g_send, g_recv, b_send, b_recv, s_send, s_recv, r_send, r_recv, done,
+):
+    me = lax.axis_index("ep")
+    mine = lax.axis_index("tp")
+    slices = length // heads
+    bits = []
+    bit = groups // 2
+    while bit >= 1:
+        bits.append(bit)
+        bit //= 2
+    barrier = pltpu.get_barrier_semaphore()
+    for k in range(1, length):
+        pl.semaphore_signal(
+            barrier, inc=1, device_id={"ep": lax.rem(me + k, length)},
+            device_id_type=pl.DeviceIdType.MESH,
+        )
+    for bit in bits:
+        pl.semaphore_signal(
+            barrier, inc=1, device_id={"tp": flipped(mine, bit)},
+            device_id_type=pl.DeviceIdType.MESH,
+        )
+    pl.semaphore_wait(barrier, length - 1 + len(bits))
+
+    pending = []
+    far = {"tp": flipped(mine, bits[0])}
+    own = remote(sent_ref.at[me], held.at[mine, me], g_send.at[0], g_recv.at[0], far)
+    own.start()
+    pending.append(own)
+    for k in range(1, length):
+        to = lax.rem(me + k, length)
+        copy = remote(
+            sent_ref.at[to], held.at[mine, me], d_send.at[k], d_recv.at[k], {"ep": to}
+        )
+        copy.start()
+        pending.append(copy)
+    held[mine, me] = sent_ref[me]
+
+    span_kernel(heads, q_ref, k_ref, v_ref, w_ref, f_ref, x_ref, s_ref, pay, loc_ref, eff_ref)
+
+    for k in range(1, length):
+        source = lax.rem(me + length - k, length)
+        block = held.at[mine, source]
+        remote(block, block, d_send.at[k], d_recv.at[k], {"ep": source}).wait_recv()
+        copy = remote(block, block, g_send.at[k], g_recv.at[k], far)
+        copy.start()
+        pending.append(copy)
+    for k in range(1, length):
+        to = lax.rem(me + k, length)
+        copy = remote(pay.at[to // slices], came.at[me], s_send.at[k], s_recv.at[k], {"ep": to})
+        copy.start()
+        pending.append(copy)
+    came[me] = pay[me // slices]
+    spot = 0
+    for bit in bits[1:]:
+        block = held.at[mine]
+        copy = remote(block, block, b_send.at[spot], b_recv.at[spot], {"tp": flipped(mine, bit)})
+        copy.start()
+        pending.append(copy)
+        spot += 1
+    for k in range(1, length):
+        source = lax.rem(me + length - k, length)
+        remote(
+            pay.at[0], came.at[source], s_send.at[k], s_recv.at[k], {"ep": source}
+        ).wait_recv()
+    fold_kernel(came, states)
+    head = me // slices
+    prior[head] = states[me]
+    for i in range(1, heads):
+        to = lax.rem(me + i * slices, length)
+        copy = remote(states.at[to], prior.at[head], r_send.at[i], r_recv.at[i], {"ep": to})
+        copy.start()
+        pending.append(copy)
+
+    for k in range(length):
+        source = lax.rem(me + length - k, length)
+        block = held.at[flipped(mine, bits[0]), source]
+        remote(block, block, g_send.at[k], g_recv.at[k], far).wait_recv()
+    have = [flipped(mine, bits[0])]
+    spot = 0
+    later = len(bits) - 1
+    for step, bit in enumerate(bits[1:]):
+        side = {"tp": flipped(mine, bit)}
+        for i, index in enumerate(have):
+            block = held.at[index]
+            at = later + (2 ** (step + 1) - 2 - step) + i
+            copy = remote(block, block, b_send.at[at], b_recv.at[at], side)
+            copy.start()
+            pending.append(copy)
+        arrived = []
+        for i, index in enumerate([mine] + have):
+            at = step if i == 0 else later + (2 ** (step + 1) - 2 - step) + i - 1
+            there = flipped(index, bit)
+            block = held.at[there]
+            remote(block, block, b_send.at[at], b_recv.at[at], side).wait_recv()
+            arrived.append(there)
+        have = have + arrived
+    whole = pltpu.make_async_copy(held, out_ref, done)
+    whole.start()
+    for i in range(1, heads):
+        source = lax.rem(me + length - i * slices, length)
+        remote(
+            states.at[0], prior.at[source // slices], r_send.at[i], r_recv.at[i], {"ep": source}
+        ).wait_recv()
+    prior_ref[...] = prior[...]
+    for copy in pending:
+        copy.wait_send()
+    whole.wait()
 
 
 def project_kernel(heads, loc_ref, eff_ref, state_ref, gate_ref, gain_ref, weight_ref, out_ref, normed):
@@ -313,21 +440,46 @@
         2 * tokens * experts * share * width,
         "dispatch",
     )(latter_micro_entries, specialist_scaling_vector[None], selected_specialists)
-    arrived = lax.all_to_all(
-        sent.reshape(experts, share, width), "ep", split_axis=0, concat_axis=0, tiled=True
-    )
-
-    offset, mapping, located, effect = call(
-        functools.partial(span_kernel, heads),
-        (
+    vmem = pl.BlockSpec(memory_space=pltpu.VMEM)
+    more = max(1, groups - 2)
+    dma = pltpu.SemaphoreType.DMA
+    pieces, prior, located, effect = pl.pallas_call(
+        functools.partial(mix_kernel, heads, length, groups),
+        out_shape=(
+            shape((groups, experts, share, width), BF),
             shape((heads, dk, dv), BF),
-            shape((heads, dk, dk), BF),
             shape((rows, heads * dv), F32),
             shape((rows, heads * dk), BF),
         ),
-        12 * 10**9,
-        "spans",
+        in_specs=[vmem] * 8,
+        out_specs=(pl.BlockSpec(memory_space=pl.ANY), vmem, vmem, vmem),
+        scratch_shapes=[
+            pltpu.VMEM((groups, experts, share, width), BF),
+            pltpu.VMEM((heads, dk, dv + dk), BF),
+            pltpu.VMEM((length, dk, dv + dk), BF),
+            pltpu.VMEM((length, dk, dv), BF),
+            pltpu.VMEM((heads, dk, dv), BF),
+            dma((length,)),
+            dma((length,)),
+            dma((length,)),
+            dma((length,)),
+            dma((more,)),
+            dma((more,)),
+            dma((length,)),
+            dma((length,)),
+            dma((heads,)),
+            dma((heads,)),
+            dma,
+        ],
+        name="mix",
+        cost_estimate=pl.CostEstimate(
+            flops=10**10, bytes_accessed=1 << 22, transcendentals=0
+        ),
+        compiler_params=pltpu.CompilerParams(
+            vmem_limit_bytes=LIMIT, collective_id=0, has_side_effects=True
+        ),
     )(
+        sent.reshape(experts, share, width),
         initial_micro_probes,
         initial_micro_lookup_keys,
         initial_micro_payloads,
@@ -337,7 +489,6 @@
         channel_fading_speed[None],
     )
 
-    pieces = gather_all(arrived.reshape(experts * share, width), groups)
     partial_sums = experts_of(
         pieces.reshape(groups * experts * share, width),
         specialist_switch_weights,
@@ -346,22 +497,6 @@
         groups,
     )
 
-    slices = length // heads
-    cols = dv // slices
-    cut = jnp.transpose(offset.reshape(heads, dk, slices, cols), (0, 2, 1, 3)).reshape(
-        length, dk, cols
-    )
-    copied = jnp.broadcast_to(mapping[:, None], (heads, slices, dk, dk)).reshape(length, dk, dk)
-    spans = lax.all_to_all(
-        jnp.concatenate([copied, cut], axis=2), "ep", split_axis=0, concat_axis=0, tiled=True
-    )
-    befores = call(
-        fold_kernel, shape((length, dk, cols), BF), length * 4 * dk * dk * cols, "fold"
-    )(spans)
-    prior = lax.all_to_all(befores, "ep", split_axis=0, concat_axis=0, tiled=True)
-    prior = jnp.transpose(prior.reshape(heads, slices, dk, cols), (0, 2, 1, 3)).reshape(
-        heads, dk, dv
-    )
     projected = call(
         functools.partial(project_kernel, heads),
         shape((rows, result_mapping_weights.shape[1]), BF),

time: 145 us -> 118 us (0.81)
  Pallas kernels: 30.5 us -> 61.7 us
  blocking collectives: 21.8 us -> 0 us
  waiting for transfers between devices: 49.3 us -> 29 us
  starting transfers between devices: 16.9 us -> 8.25 us
  local copies, waits for them, and re-layouts: 17.5 us -> 13.6 us
  other arithmetic: 7.24 us -> 3.6 us
    pallas_call x2 -> x1, Pallas kernels: 8.81 us -> 40.1 us  [local(): pl.pallas_call(functools.partial(mix_kernel, heads, length, groups), out_...]
    all_to_all x1 -> x0, blocking collectives: 21.8 us -> none  [local(): lax.all_to_all(sent.reshape(experts, share, width), 'ep', split_axis=0, c...]
    all_to_all x2 -> x0, waiting for transfers between devices: 15.6 us -> none  [the longest x1 8.3 us: local(): lax.all_to_all(jnp.concatenate([copied, cut], axis=2), 'ep', split_axis=0...]
    all_to_all x2 -> x0, starting transfers between devices: 8 us -> none  [the longest x1 4.37 us: local(): lax.all_to_all(jnp.concatenate([copied, cut], axis=2), 'ep', split_axis=0...]
    ppermute x8 -> x6, waiting for transfers between devices: 19.2 us -> 15.9 us  [swap(): return lax.ppermute(value, 'tp', [(j, j ^ bit) for j in range(size)])]
    pallas_call x2 -> x0, local copies, waits for them, and re-layouts: 2.75 us -> none  [the longest x1 1.73 us: local(): call(fold_kernel, shape((length, dk, cols), BF), length * 4 * dk * dk * c...]
    unnamed x20 -> x12, local copies, waits for them, and re-layouts: 6.39 us -> 8.37 us
    ppermute x8 -> x6, starting transfers between devices: 5.41 us -> 3.61 us  [swap(): return lax.ppermute(value, 'tp', [(j, j ^ bit) for j in range(size)])]
  transfers between devices with their start and end apart: 11 -> 7, of which waited for: 7 -> 5; matrix products, arithmetic and copies ran while one was open for 12% -> 5% of each run, Pallas kernels for 9% -> 3%
where the time goes in v2:
time: 118 us; the launch traced here: 117 us
  Pallas kernels  61.7 us (52%)
  waiting for transfers between devices  29 us (25%)
  local copies, waits for them, and re-layouts  13.6 us (12%)
  starting transfers between devices  8.25 us (7%)
  other arithmetic  3.6 us (3%)
    pallas_call x1, Pallas kernels, local(): pl.pallas_call(functools.partial(mix_kernel, heads, length, groups), out_...  40.1 us
    ppermute x6, waiting for transfers between devices, swap(): return lax.ppermute(value, 'tp', [(j, j ^ bit) for j in range(size)])  15.9 us
    all_to_all x1, waiting for transfers between devices, local(): lax.all_to_all(summed, 'ep', split_axis=0, concat_axis=0, tiled=True)  13.1 us
    pallas_call x1, Pallas kernels, experts_of(): pl.pallas_call(expert_kernel, grid=(ff // tile,), in_specs=[pl.BlockSpec(...  12.5 us
    unnamed x12, local copies, waits for them, and re-layouts  8.37 us
    all_to_all x1, starting transfers between devices, local(): lax.all_to_all(summed, 'ep', split_axis=0, concat_axis=0, tiled=True)  4.65 us
    squeeze x4, local copies, waits for them, and re-layouts, scatter_sum(): give = lax.dynamic_index_in_dim(pairs, 1 - upper, 1, keepdims=False)  4.06 us
    pallas_call x1, Pallas kernels, local(): call(functools.partial(project_kernel, heads), shape((rows, result_mappin...  4.02 us
  transfers between devices with their start and end apart: 7, of which 5 were waited for; matrix products, arithmetic and copies ran while one was open for 5% of the time, Pallas kernels for 3%

profile of v2, /device:TPU:0, one launch (start us, length us, event | category | flops | bytes accessed | tf_op | source)
XLA Modules:
  0.0 117.0 jit_solution(8206098691680090027)
XLA Ops:
  0.6 1.4 %copy.36.route_ref = s32[128,2]{1,0:T(8,128)} copy(s32[128,2]{0,1:T(2,128)} %param.29) | data formatting | bytes 2048 | tf_op args[12]
  2.0 1.5 %copy.37.w_ref = f32[256,4]{1,0:T(8,128)} copy(f32[256,4]{0,1:T(4,128)} %param.21) | data formatting | bytes 8192 | tf_op args[4]
  3.5 1.5 %copy.38.f_ref = f32[256,4]{1,0:T(8,128)} copy(f32[256,4]{0,1:T(4,128)} %param.22) | data formatting | bytes 8192 | tf_op args[5]
  5.0 1.5 %copy.39.x_ref = f32[256,4]{1,0:T(8,128)} copy(f32[256,4]{0,1:T(4,128)} %param.23) | data formatting | bytes 8192 | tf_op args[6]
  6.5 2.6 %dispatch.1 = bf16[128,2048]{1,0:T(8,128)(2,1)} custom-call(bf16[128,2048]{1,0:T(8,128)(2,1)} %x_ref.2, f32[1,2048]{1,0:T(1,128)} %bitcast.57, s32[128,2]{1,0:T(8,128)} %copy.36.route_ref), custom_call_target="tpu_custom_call" | custom-call | flops 67108864 | bytes 2097152 | tf_op jit(solution)/shard_map/dispatch/pallas_call | solution.py:437
  9.1 40.1 %mix.1 = (bf16[4,8,16,2048]{3,2,1,0:T(8,128)(2,1)}, bf16[4,128,128]{2,1,0:T(8,128)(2,1)}, f32[256,512]{1,0:T(8,128)}, bf16[256,512]{1,0:T(8,128)(2,1)}) custom-call(bf16[8,16,2048]{2,1,0:T(8,128)(2,1)} %bitcast.55, bf16[256,512]{1,0:T(8,128)(2,1)} %q_ref.1, bf16[256,512]{1,0:T(8,128)(2,1)} %k_ref.1, bf16[256,512]{1,0:T(8,128)(2,1)} %v_ref.1, ...), custom_call_target="tpu_custom_call" | custom-call | flops 10000000000 | bytes 4194304 | tf_op jit(solution)/shard_map/mix/pallas_call | solution.py:446
  49.2 12.5 %experts.1 = bf16[4,512,512]{2,1,0:T(8,128)(2,1)} custom-call(bf16[512,2048]{1,0:T(8,128)(2,1)} %bitcast.60, bf16[1,2048,1024]{2,1,0:T(8,128)(2,1)} %g_ref.1, bf16[1,2048,1024]{2,1,0:T(8,128)(2,1)} %u_ref.1, bf16[1,1024,2048]{2,1,0:T(8,128)(2,1)} %d_ref.1), custom_call_target="tpu_custom_call" | custom-call | flops 6442450944 | bytes 12582912 | tf_op jit(solution)/shard_map/experts/pallas_call | solution.py:352
  61.7 1.3 %dynamic-slice_bitcast_fusion = bf16[2,512,512]{2,1,0:T(8,128)(2,1)S(1)} fusion(bf16[2,2,512,512]{3,2,1,0:T(8,128)(2,1)} %bitcast.49, s32[]{:T(128)S(6)} %select_n.74), kind=kLoop, calls=%fused_computation.5 | loop fusion | bytes 2097156 | tf_op jit(solution)/shard_map/jit(dynamic_index_in_dim)/squeeze | solution.py:384
  63.0 0.1 collective-permute-start.2
  63.1 2.6 %collective-permute-done.2 = bf16[2,512,512]{2,1,0:T(8,128)(2,1)S(1)} collective-permute-done((bf16[2,512,512]{2,1,0:T(8,128)(2,1)S(1)}, bf16[2,512,512]{2,1,0:T(8,128)(2,1)S(1)}, u32[]{:S(2)}, u32[]{:S(2)}) %collective-permute-start.2) | collective-permute-done | bytes 1048608 | tf_op jit(solution)/shard_map/ppermute | solution.py:373
  65.7 1.5 %fusion = bf16[2,512,512]{2,1,0:T(8,128)(2,1)S(1)} fusion(bf16[2,512,512]{2,1,0:T(8,128)(2,1)S(1)} %collective-permute-done.2, bf16[2,2,512,512]{3,2,1,0:T(8,128)(2,1)} %bitcast.50, s32[]{:T(128)S(6)} %select_n.73), kind=kLoop, calls=%fused_computation.1 | loop fusion | flops 2097152 | bytes 3145732 | tf_op jit(solution)/shard_map/convert_element_type | solution.py:386
  67.2 0.9 constant_dynamic-slice_fusion
  68.1 1.4 %collective-permute-start.3 = (bf16[1,512,512]{2,1,0:T(8,128)(2,1)}, bf16[1,512,512]{2,1,0:T(8,128)(2,1)S(1)}, u32[]{:S(2)}, u32[]{:S(2)}) collective-permute-start(bf16[1,512,512]{2,1,0:T(8,128)(2,1)} %constant_dynamic-slice_fusion), channel_id=1, source_target_pairs={{0,2},{1,3},{2,0},{3,1},{4,6},{5,7},{6,4},{7,5},{8,10},{9,11},{10,... | collective-permute-start | bytes 1572872 | tf_op jit(solution)/shard_map/ppermute | solution.py:373
  69.4 4.0 %project.1 = bf16[256,2048]{1,0:T(8,128)(2,1)} custom-call(f32[256,512]{1,0:T(8,128)} %get-tuple-element.6.loc_ref, bf16[256,512]{1,0:T(8,128)(2,1)} %get-tuple-element.7.eff_ref, bf16[4,128,128]{2,1,0:T(8,128)(2,1)} %get-tuple-element.8.state_ref, bf16[256,512]{1,0:T(8,128)(2,1)} %gate_ref.1, f32[1,128]{1,0:T(1,128)} %bitcast.58, bf16[512,2048]{1,0:T(8,128)(2,1)} %weight_ref.1), custom_call_target="tpu_custom_call" | custom-call | flops 536870912 | bytes 2097152 | tf_op jit(solution)/shard_map/project/pallas_call | solution.py:500
  73.5 1.9 %dynamic-slice_bitcast_fusion.1 = bf16[2,64,2048]{2,1,0:T(8,128)(2,1)} fusion(bf16[2,2,64,2048]{3,2,1,0:T(8,128)(2,1)} %bitcast.47, s32[]{:T(128)S(6)} %select_n.74), kind=kLoop, calls=%fused_computation.8 | loop fusion | bytes 1048580 | tf_op jit(solution)/shard_map/jit(dynamic_index_in_dim)/squeeze | solution.py:384
  75.3 0.0 copy-start.2
  75.3 0.0 copy-start
  75.3 0.0 collective-permute-start
  75.3 6.9 %collective-permute-done.3 = bf16[1,512,512]{2,1,0:T(8,128)(2,1)S(1)} collective-permute-done((bf16[1,512,512]{2,1,0:T(8,128)(2,1)}, bf16[1,512,512]{2,1,0:T(8,128)(2,1)S(1)}, u32[]{:S(2)}, u32[]{:S(2)}) %collective-permute-start.3) | collective-permute-done | bytes 524320 | tf_op jit(solution)/shard_map/ppermute | solution.py:373
  82.2 0.1 add_convert_fusion
  82.4 0.9 copy.41
  83.3 4.6 %all-to-all-start = ((bf16[8,64,512]{2,1,0:T(8,128)(2,1)}), bf16[8,64,512]{2,1,0:T(8,128)(2,1)S(1)}, u32[]{:S(2)}, u32[]{:S(2)}) async-start(bf16[8,64,512]{2,1,0:T(8,128)(2,1)} %bitcast.14), calls=%async_computation | async-start | bytes 1048576 | tf_op jit(solution)/shard_map/all_to_all | solution.py:519
  87.9 0.0 copy-done.2
  87.9 0.7 copy.43.score_ref
  88.6 0.0 collective-permute-done
  88.6 0.0 copy-done
  88.6 0.1 fusion.1
  88.8 13.1 %all-to-all-done = bf16[8,64,512]{2,1,0:T(8,128)(2,1)S(1)} async-done(((bf16[8,64,512]{2,1,0:T(8,128)(2,1)}), bf16[8,64,512]{2,1,0:T(8,128)(2,1)S(1)}, u32[]{:S(2)}, u32[]{:S(2)}) %all-to-all-start) | async-done | bytes 524320 | tf_op jit(solution)/shard_map/all_to_all | solution.py:519
  101.9 0.0 copy-start.1
  101.9 0.8 copy-done.1
  102.7 2.5 %combine.1 = bf16[128,512]{1,0:T(8,128)(2,1)} custom-call(bf16[512,512]{1,0:T(8,128)(2,1)} %bitcast.51, s32[128,2]{1,0:T(8,128)} %copy.36.route_ref, f32[128,2]{1,0:T(8,128)} %copy.43.score_ref), custom_call_target="tpu_custom_call" | custom-call | flops 134217728 | bytes 2097152 | tf_op jit(solution)/shard_map/combine/pallas_call | solution.py:520
  105.2 1.3 %collective-permute-start.4 = (bf16[1,128,512]{2,1,0:T(8,128)(2,1)}, bf16[1,128,512]{2,1,0:T(8,128)(2,1)S(1)}, u32[]{:S(2)}, u32[]{:S(2)}) collective-permute-start(bf16[1,128,512]{2,1,0:T(8,128)(2,1)} %bitcast.56), channel_id=1, source_target_pairs={{0,2},{1,3},{2,0},{3,1},{4,6},{5,7},{6,4},{7,5},{8,10},{9,11},{10,... | collective-permute-start | bytes 393224 | tf_op jit(solution)/shard_map/ppermute | solution.py:373
  106.5 0.8 collective-permute-start.1
  107.3 4.5 %collective-permute-done.4 = bf16[1,128,512]{2,1,0:T(8,128)(2,1)S(1)} collective-permute-done((bf16[1,128,512]{2,1,0:T(8,128)(2,1)}, bf16[1,128,512]{2,1,0:T(8,128)(2,1)S(1)}, u32[]{:S(2)}, u32[]{:S(2)}) %collective-permute-start.4) | collective-permute-done | bytes 131104 | tf_op jit(solution)/shard_map/ppermute | solution.py:373
  111.7 0.9 select_bitcast_fusion.3
  112.7 0.1 collective-permute-start.5
  112.8 2.0 %collective-permute-done.1 = bf16[1,64,2048]{2,1,0:T(8,128)(2,1)S(1)} collective-permute-done((bf16[1,64,2048]{2,1,0:T(8,128)(2,1)S(1)}, bf16[1,64,2048]{2,1,0:T(8,128)(2,1)S(1)}, u32[]{:S(2)}, u32[]{:S(2)}) %collective-permute-start.1) | collective-permute-done | bytes 262176 | tf_op jit(solution)/shard_map/ppermute | solution.py:373
  114.8 0.8 fusion.2
  115.5 0.0 collective-permute-done.5
  115.6 0.1 pad_maximum_fusion
  115.7 0.3 copy.45
  116.0 1.0 copy.46
  (4 shorter events, 0.1 us)
Async XLA Ops:
  63.0 2.7 %collective-permute-start.2 = (bf16[2,512,512]{2,1,0:T(8,128)(2,1)S(1)}, bf16[2,512,512]{2,1,0:T(8,128)(2,1)S(1)}, u32[]{:S(2)}, u32[]{:S(2)}) collective-permute-start(bf16[2,512,512]{2,1,0:T(8,128)(2,1)S(1)} %dynamic-slice_bitcast_fusion), channel_id=1, source_target_pairs={{0,1},{1,0},{2,3},{3,2},{4,5},{5,4},{6,7},{7,6},{8,9},{9,8},{10,11... | collective-permute-start | bytes 3145736 | tf_op jit(solution)/shard_map/ppermute | solution.py:373
  68.1 14.2 %collective-permute-start.3 = (bf16[1,512,512]{2,1,0:T(8,128)(2,1)}, bf16[1,512,512]{2,1,0:T(8,128)(2,1)S(1)}, u32[]{:S(2)}, u32[]{:S(2)}) collective-permute-start(bf16[1,512,512]{2,1,0:T(8,128)(2,1)} %constant_dynamic-slice_fusion), channel_id=1, source_target_pairs={{0,2},{1,3},{2,0},{3,1},{4,6},{5,7},{6,4},{7,5},{8,10},{9,11},{10,... | collective-permute-start | bytes 1572872 | tf_op jit(solution)/shard_map/ppermute | solution.py:373
  75.3 12.6 %copy-start.2 = (f32[128,2]{0,1:T(2,128)S(1)}, f32[128,2]{0,1:T(2,128)}, u32[]{:S(2)}) copy-start(f32[128,2]{0,1:T(2,128)} %param.30) | copy-start | bytes 3076
  75.3 13.3 %copy-start = (bf16[256,2048]{1,0:T(8,128)(2,1)S(1)}, bf16[256,2048]{1,0:T(8,128)(2,1)}, u32[]{:S(2)}) copy-start(bf16[256,2048]{1,0:T(8,128)(2,1)} %project.1) | copy-start | bytes 3145732
  75.3 13.3 %collective-permute-start = (bf16[2,64,2048]{2,1,0:T(8,128)(2,1)}, bf16[2,64,2048]{2,1,0:T(8,128)(2,1)S(1)}, u32[]{:S(2)}, u32[]{:S(2)}) collective-permute-start(bf16[2,64,2048]{2,1,0:T(8,128)(2,1)} %dynamic-slice_bitcast_fusion.1), channel_id=1, source_target_pairs={{0,1},{1,0},{2,3},{3,2},{4,5},{5,4},{6,7},{7,6},{8,9},{9,8},{10,11... | collective-permute-start | bytes 1572872 | tf_op jit(solution)/shard_map/ppermute | solution.py:373
  83.3 18.6 %all-to-all-start = ((bf16[8,64,512]{2,1,0:T(8,128)(2,1)}), bf16[8,64,512]{2,1,0:T(8,128)(2,1)S(1)}, u32[]{:S(2)}, u32[]{:S(2)}) async-start(bf16[8,64,512]{2,1,0:T(8,128)(2,1)} %bitcast.14), calls=%async_computation | async-start | bytes 1048576 | tf_op jit(solution)/shard_map/all_to_all | solution.py:519
  101.9 0.8 copy-start.1
  105.2 6.6 %collective-permute-start.4 = (bf16[1,128,512]{2,1,0:T(8,128)(2,1)}, bf16[1,128,512]{2,1,0:T(8,128)(2,1)S(1)}, u32[]{:S(2)}, u32[]{:S(2)}) collective-permute-start(bf16[1,128,512]{2,1,0:T(8,128)(2,1)} %bitcast.56), channel_id=1, source_target_pairs={{0,2},{1,3},{2,0},{3,1},{4,6},{5,7},{6,4},{7,5},{8,10},{9,11},{10,... | collective-permute-start | bytes 393224 | tf_op jit(solution)/shard_map/ppermute | solution.py:373
  106.5 8.3 %collective-permute-start.1 = (bf16[1,64,2048]{2,1,0:T(8,128)(2,1)S(1)}, bf16[1,64,2048]{2,1,0:T(8,128)(2,1)S(1)}, u32[]{:S(2)}, u32[]{:S(2)}) collective-permute-start(bf16[1,64,2048]{2,1,0:T(8,128)(2,1)S(1)} %constant_dynamic-slice_fusion.1), channel_id=1, source_target_pairs={{0,2},{1,3},{2,0},{3,1},{4,6},{5,7},{6,4},{7,5},{8,10},{9,11},{10,... | collective-permute-start | bytes 786440 | tf_op jit(solution)/shard_map/ppermute | solution.py:373
  112.7 2.8 %collective-permute-start.5 = (bf16[2,128,512]{2,1,0:T(8,128)(2,1)S(1)}, bf16[2,128,512]{2,1,0:T(8,128)(2,1)S(1)}, u32[]{:S(2)}, u32[]{:S(2)}) collective-permute-start(bf16[2,128,512]{2,1,0:T(8,128)(2,1)S(1)} %maximum_bitcast_fusion), channel_id=1, source_target_pairs={{0,1},{1,0},{2,3},{3,2},{4,5},{5,4},{6,7},{7,6},{8,9},{9,8},{10,11... | collective-permute-start | bytes 786440 | tf_op jit(solution)/shard_map/ppermute | solution.py:373

commit v3 on v2

--- a/solution.py
+++ b/solution.py
@@ -180,23 +180,23 @@
 
     pending = []
     far = {"tp": flipped(mine, bits[0])}
-    own = remote(sent_ref.at[me], held.at[mine, me], g_send.at[0], g_recv.at[0], far)
+    own = remote(sent_ref.at[me], held.at[me, mine], g_send.at[0], g_recv.at[0], far)
     own.start()
     pending.append(own)
     for k in range(1, length):
         to = lax.rem(me + k, length)
         copy = remote(
-            sent_ref.at[to], held.at[mine, me], d_send.at[k], d_recv.at[k], {"ep": to}
+            sent_ref.at[to], held.at[me, mine], d_send.at[k], d_recv.at[k], {"ep": to}
         )
         copy.start()
         pending.append(copy)
-    held[mine, me] = sent_ref[me]
+    held[me, mine] = sent_ref[me]
 
     span_kernel(heads, q_ref, k_ref, v_ref, w_ref, f_ref, x_ref, s_ref, pay, loc_ref, eff_ref)
 
     for k in range(1, length):
         source = lax.rem(me + length - k, length)
-        block = held.at[mine, source]
+        block = held.at[source, mine]
         remote(block, block, d_send.at[k], d_recv.at[k], {"ep": source}).wait_recv()
         copy = remote(block, block, g_send.at[k], g_recv.at[k], far)
         copy.start()
@@ -209,7 +209,7 @@
     came[me] = pay[me // slices]
     spot = 0
     for bit in bits[1:]:
-        block = held.at[mine]
+        block = held.at[:, mine]
         copy = remote(block, block, b_send.at[spot], b_recv.at[spot], {"tp": flipped(mine, bit)})
         copy.start()
         pending.append(copy)
@@ -230,7 +230,7 @@
 
     for k in range(length):
         source = lax.rem(me + length - k, length)
-        block = held.at[flipped(mine, bits[0]), source]
+        block = held.at[source, flipped(mine, bits[0])]
         remote(block, block, g_send.at[k], g_recv.at[k], far).wait_recv()
     have = [flipped(mine, bits[0])]
     spot = 0
@@ -238,7 +238,7 @@
     for step, bit in enumerate(bits[1:]):
         side = {"tp": flipped(mine, bit)}
         for i, index in enumerate(have):
-            block = held.at[index]
+            block = held.at[:, index]
             at = later + (2 ** (step + 1) - 2 - step) + i
             copy = remote(block, block, b_send.at[at], b_recv.at[at], side)
             copy.start()
@@ -247,7 +247,7 @@
         for i, index in enumerate([mine] + have):
             at = step if i == 0 else later + (2 ** (step + 1) - 2 - step) + i - 1
             there = flipped(index, bit)
-            block = held.at[there]
+            block = held.at[:, there]
             remote(block, block, b_send.at[at], b_recv.at[at], side).wait_recv()
             arrived.append(there)
         have = have + arrived
@@ -308,17 +308,124 @@
     out_ref[...] = mm_tn(taken.astype(BF), normed).astype(BF)
 
 
-def combine_kernel(experts, capacity, y_ref, route_ref, score_ref, out_ref):
+def return_kernel(
+    length, groups, capacity,
+    part_ref, route_ref, score_ref, out_ref,
+    gots, sums, final, came, spread,
+    l_send, l_recv, r_send, r_recv, g_send, g_recv,
+):
+    me = lax.axis_index("ep")
+    mine = lax.axis_index("tp")
+    levels = len(gots)
+    bits = [1 << l for l in range(levels)]
+    barrier = pltpu.get_barrier_semaphore()
+    for k in range(1, length):
+        pl.semaphore_signal(
+            barrier, inc=1, device_id={"ep": lax.rem(me + k, length)},
+            device_id_type=pl.DeviceIdType.MESH,
+        )
+    for bit in bits:
+        pl.semaphore_signal(
+            barrier, inc=1, device_id={"tp": flipped(mine, bit)},
+            device_id_type=pl.DeviceIdType.MESH,
+        )
+    pl.semaphore_wait(barrier, length - 1 + levels)
+    pending = []
+
+    def give(level, k):
+        bit = bits[level]
+        other = 1 - (mine // bit) % 2
+        source = part_ref if level == 0 else sums[level - 1]
+        at = level * length + k
+        chunk = lax.rem(me + k, length)
+        return remote(
+            source.at[:, other, chunk], gots[level].at[:, chunk],
+            l_send.at[at], l_recv.at[at], {"tp": flipped(mine, bit)},
+        )
+
+    def back(k):
+        to = lax.rem(me + k, length)
+        return remote(final.at[to], came.at[me], r_send.at[k], r_recv.at[k], {"ep": to})
+
+    def begin(copy):
+        copy.start()
+        pending.append(copy)
+
+    order = list(range(1, length)) + [0]
+    for k in order:
+        begin(give(0, k))
+    for level in range(levels):
+        upper = (mine // bits[level]) % 2
+        source = part_ref if level == 0 else sums[level - 1]
+        before = None
+        for k in order:
+            chunk = lax.rem(me + k, length)
+            give(level, k).wait_recv()
+            total = (
+                source[:, upper, chunk].astype(F32) + gots[level][:, chunk].astype(F32)
+            ).astype(BF)
+            if level + 1 < levels:
+                width = total.shape[0] // 2
+                for i in range(width):
+                    for j in range(2):
+                        sums[level][i, j, chunk] = total[2 * i + j]
+                if before is not None:
+                    begin(give(level + 1, before))
+            elif k == 0:
+                came[me] = total[0]
+            else:
+                final[chunk] = total[0]
+                if before is not None:
+                    begin(back(before))
+            before = k
+            if level + 1 == levels and k == order[-2]:
+                last = k
+        if level + 1 < levels:
+            begin(give(level + 1, before))
+        elif length > 1:
+            begin(back(last))
+
     route = route_ref[...]
     tokens = route.shape[0]
     score = score_ref[...]
     score = score / jnp.sum(score, axis=1, keepdims=True)
-    slots = lax.broadcasted_iota(jnp.int32, (tokens, experts * capacity), 1)
-    total = jnp.zeros(out_ref.shape, F32)
-    for j, place in enumerate(slot_places(route, experts)):
+    slots = lax.broadcasted_iota(jnp.int32, (tokens, length * capacity), 1)
+    picks = []
+    for j, place in enumerate(slot_places(route, length)):
         target = route[:, j : j + 1] * capacity + place
-        total = total + score[:, j : j + 1] * mm((slots == target).astype(BF), y_ref[...])
-    out_ref[...] = total.astype(BF)
+        picks.append((slots == target).astype(BF))
+    for k in range(1, length):
+        source = lax.rem(me + length - k, length)
+        remote(
+            final.at[source], came.at[source], r_send.at[k], r_recv.at[k], {"ep": source}
+        ).wait_recv()
+    values = came[...].reshape(length * capacity, came.shape[2])
+    total = functools.reduce(
+        jnp.add, [score[:, j : j + 1] * mm(pick, values) for j, pick in enumerate(picks)]
+    )
+    spread[mine] = total.astype(BF)
+    out_ref[:, : spread.shape[2]] = spread[mine]
+    have = [mine]
+    at = 0
+    for bit in reversed(bits):
+        side = {"tp": flipped(mine, bit)}
+        arrived = []
+        for index in have:
+            begin(remote(spread.at[index], spread.at[index], g_send.at[at], g_recv.at[at], side))
+            at += 1
+        at -= len(have)
+        for index in have:
+            there = flipped(index, bit)
+            block = spread.at[there]
+            remote(block, block, g_send.at[at], g_recv.at[at], side).wait_recv()
+            arrived.append(there)
+            at += 1
+        have = have + arrived
+    cols = spread.shape[2]
+    for g in range(groups):
+        out_ref[:, g * cols : (g + 1) * cols] = spread[g]
+    for copy in pending:
+        copy.wait_send()
 
 
 def expert_kernel(x_ref, g_ref, u_ref, d_ref, out_ref, acc):
@@ -386,20 +493,6 @@
         rest = (keep.astype(F32) + got.astype(F32)).astype(BF)
         bit *= 2
     return rest[0]
-
-
-def gather_all(value, size):
-    mine = lax.axis_index("tp")
-    bit = size // 2
-    rest = value[None]
-    while bit >= 1:
-        got = swap(rest, bit, size)
-        upper = (mine // bit) % 2 == 1
-        low = jnp.where(upper, got, rest)
-        high = jnp.where(upper, rest, got)
-        rest = jnp.stack([low, high], axis=1).reshape((2 * rest.shape[0],) + value.shape)
-        bit //= 2
-    return rest
 
 
 def local(
@@ -446,7 +539,7 @@
     pieces, prior, located, effect = pl.pallas_call(
         functools.partial(mix_kernel, heads, length, groups),
         out_shape=(
-            shape((groups, experts, share, width), BF),
+            shape((experts, groups, share, width), BF),
             shape((heads, dk, dv), BF),
             shape((rows, heads * dv), F32),
             shape((rows, heads * dk), BF),
@@ -454,7 +547,7 @@
         in_specs=[vmem] * 8,
         out_specs=(pl.BlockSpec(memory_space=pl.ANY), vmem, vmem, vmem),
         scratch_shapes=[
-            pltpu.VMEM((groups, experts, share, width), BF),
+            pltpu.VMEM((experts, groups, share, width), BF),
             pltpu.VMEM((heads, dk, dv + dk), BF),
             pltpu.VMEM((length, dk, dv + dk), BF),
             pltpu.VMEM((length, dk, dv), BF),
@@ -513,21 +606,39 @@
     )
     mixer_out = scatter_sum(projected.reshape(groups, rows // groups, -1), groups)
 
-    summed = scatter_sum(partial_sums, groups)
-    summed = summed.reshape(groups, experts, share, width // groups)
-    summed = jnp.transpose(summed, (1, 0, 2, 3)).reshape(experts, capacity, width // groups)
-    returned = lax.all_to_all(summed, "ep", split_axis=0, concat_axis=0, tiled=True)
-    combined = call(
-        functools.partial(combine_kernel, experts, capacity),
-        shape((tokens, width // groups), BF),
-        4 * tokens * experts * capacity * (width // groups),
-        "combine",
+    cols = width // groups
+    levels = groups.bit_length() - 1
+    halves = [groups >> (l + 1) for l in range(levels)]
+    moe_out = pl.pallas_call(
+        functools.partial(return_kernel, length, groups, capacity),
+        out_shape=shape((tokens, width), BF),
+        in_specs=[vmem] * 3,
+        out_specs=vmem,
+        scratch_shapes=[
+            [pltpu.VMEM((n, experts, capacity, cols), BF) for n in halves],
+            [pltpu.VMEM((n // 2, 2, experts, capacity, cols), BF) for n in halves[:-1]],
+            pltpu.VMEM((experts, capacity, cols), BF),
+            pltpu.VMEM((experts, capacity, cols), BF),
+            pltpu.VMEM((groups, tokens, cols), BF),
+            dma((levels * length,)),
+            dma((levels * length,)),
+            dma((length,)),
+            dma((length,)),
+            dma((groups,)),
+            dma((groups,)),
+        ],
+        name="return",
+        cost_estimate=pl.CostEstimate(
+            flops=10**10, bytes_accessed=1 << 22, transcendentals=0
+        ),
+        compiler_params=pltpu.CompilerParams(
+            vmem_limit_bytes=LIMIT, collective_id=1, has_side_effects=True
+        ),
     )(
-        returned.reshape(experts * capacity, width // groups),
+        partial_sums.reshape(groups // 2, 2, experts, capacity, cols),
         selected_specialists,
         selected_dispatch_weights,
     )
-    moe_out = jnp.transpose(gather_all(combined, groups), (1, 0, 2)).reshape(tokens, width)
     return (mixer_out, moe_out)
 
 

time: 118 us -> 105 us (0.89)
  the two profiles are of different devices: /device:TPU:0 before, /device:TPU:11 now
where the time goes in v3:
time: 105 us
  Pallas kernels  90.9 us (87%)
  local copies, waits for them, and re-layouts  9.6 us (9%)
  starting transfers between devices  2.73 us (3%)
    pallas_call x1, Pallas kernels, local(): pl.pallas_call(functools.partial(mix_kernel, heads, length, groups), out_...  38 us
    pallas_call x1, Pallas kernels, local(): pl.pallas_call(functools.partial(return_kernel, length, groups, capacity)...  33.6 us
    pallas_call x1, Pallas kernels, experts_of(): pl.pallas_call(expert_kernel, grid=(ff // tile,), in_specs=[pl.BlockSpec(...  12.5 us
    unnamed x10, local copies, waits for them, and re-layouts  8.49 us
    pallas_call x1, Pallas kernels, local(): call(functools.partial(project_kernel, heads), shape((rows, result_mappin...  4.04 us
    ppermute x2, starting transfers between devices, swap(): return lax.ppermute(value, 'tp', [(j, j ^ bit) for j in range(size)])  2.73 us
    pallas_call x1, Pallas kernels, local(): call(functools.partial(dispatch_kernel, experts, share), shape((experts *...  2.62 us
  transfers between devices with their start and end apart: 2, of which 0 were waited for; matrix products, arithmetic and copies ran while one was open for 1% of the time, Pallas kernels for 44%

profile of v3, /device:TPU:11, one launch (start us, length us, event | category | flops | bytes accessed | tf_op | source)
XLA Modules:
  0.0 104.8 jit_solution(17614331971165270340)
XLA Ops:
  0.6 1.4 %copy.19.route_ref = s32[128,2]{1,0:T(8,128)} copy(s32[128,2]{0,1:T(2,128)} %param.29) | data formatting | bytes 2048 | tf_op args[12]
  2.1 1.5 %copy.20.w_ref = f32[256,4]{1,0:T(8,128)} copy(f32[256,4]{0,1:T(4,128)} %param.21) | data formatting | bytes 8192 | tf_op args[4]
  3.5 1.5 %copy.21.f_ref = f32[256,4]{1,0:T(8,128)} copy(f32[256,4]{0,1:T(4,128)} %param.22) | data formatting | bytes 8192 | tf_op args[5]
  5.0 1.5 %copy.22.x_ref = f32[256,4]{1,0:T(8,128)} copy(f32[256,4]{0,1:T(4,128)} %param.23) | data formatting | bytes 8192 | tf_op args[6]
  6.5 2.6 %dispatch.1 = bf16[128,2048]{1,0:T(8,128)(2,1)} custom-call(bf16[128,2048]{1,0:T(8,128)(2,1)} %x_ref.2, f32[1,2048]{1,0:T(1,128)} %bitcast.19, s32[128,2]{1,0:T(8,128)} %copy.19.route_ref), custom_call_target="tpu_custom_call" | custom-call | flops 67108864 | bytes 2097152 | tf_op jit(solution)/shard_map/dispatch/pallas_call | solution.py:530
  9.1 38.0 %mix.1 = (bf16[8,4,16,2048]{3,2,1,0:T(8,128)(2,1)}, bf16[4,128,128]{2,1,0:T(8,128)(2,1)}, f32[256,512]{1,0:T(8,128)}, bf16[256,512]{1,0:T(8,128)(2,1)}) custom-call(bf16[8,16,2048]{2,1,0:T(8,128)(2,1)} %bitcast.18, bf16[256,512]{1,0:T(8,128)(2,1)} %q_ref.1, bf16[256,512]{1,0:T(8,128)(2,1)} %k_ref.1, bf16[256,512]{1,0:T(8,128)(2,1)} %v_ref.1, ...), custom_call_target="tpu_custom_call" | custom-call | flops 10000000000 | bytes 4194304 | tf_op jit(solution)/shard_map/mix/pallas_call | solution.py:539
  47.2 0.0 copy-start.1
  47.2 4.0 %project.1 = bf16[256,2048]{1,0:T(8,128)(2,1)} custom-call(f32[256,512]{1,0:T(8,128)} %get-tuple-element.6.loc_ref, bf16[256,512]{1,0:T(8,128)(2,1)} %get-tuple-element.7.eff_ref, bf16[4,128,128]{2,1,0:T(8,128)(2,1)} %get-tuple-element.8.state_ref, bf16[256,512]{1,0:T(8,128)(2,1)} %gate_ref.1, f32[1,128]{1,0:T(1,128)} %bitcast.20, bf16[512,2048]{1,0:T(8,128)(2,1)} %weight_ref.1), custom_call_target="tpu_custom_call" | custom-call | flops 536870912 | bytes 2097152 | tf_op jit(solution)/shard_map/project/pallas_call | solution.py:593
  51.2 1.1 %dynamic-slice_bitcast_fusion = bf16[2,64,2048]{2,1,0:T(8,128)(2,1)S(1)} fusion(bf16[2,2,64,2048]{3,2,1,0:T(8,128)(2,1)} %bitcast.16, s32[]{:T(128)S(6)} %select_n.32), kind=kLoop, calls=%fused_computation.3 | loop fusion | bytes 1048580 | tf_op jit(solution)/shard_map/jit(dynamic_index_in_dim)/squeeze | solution.py:491
  52.3 1.8 %collective-permute-start = (bf16[2,64,2048]{2,1,0:T(8,128)(2,1)S(1)}, bf16[2,64,2048]{2,1,0:T(8,128)(2,1)S(1)}, u32[]{:S(2)}, u32[]{:S(2)}) collective-permute-start(bf16[2,64,2048]{2,1,0:T(8,128)(2,1)S(1)} %dynamic-slice_bitcast_fusion), channel_id=1, source_target_pairs={{0,1},{1,0},{2,3},{3,2},{4,5},{5,4},{6,7},{7,6},{8,9},{9,8},{10,11... | collective-permute-start | bytes 1572872 | tf_op jit(solution)/shard_map/ppermute | solution.py:480
  54.1 0.0 copy-done.1
  54.1 0.7 copy.25.score_ref
  54.9 0.0 copy-start
  54.9 12.5 %experts.1 = bf16[4,512,512]{2,1,0:T(8,128)(2,1)} custom-call(bf16[512,2048]{1,0:T(8,128)(2,1)} %bitcast.22, bf16[1,2048,1024]{2,1,0:T(8,128)(2,1)} %g_ref.1, bf16[1,2048,1024]{2,1,0:T(8,128)(2,1)} %u_ref.1, bf16[1,1024,2048]{2,1,0:T(8,128)(2,1)} %d_ref.1), custom_call_target="tpu_custom_call" | custom-call | flops 6442450944 | bytes 12582912 | tf_op jit(solution)/shard_map/experts/pallas_call | solution.py:459
  67.4 0.0 collective-permute-done
  67.4 0.0 copy-done
  67.4 0.1 fusion
  67.6 0.9 collective-permute-start.1
  68.5 33.6 %return.1 = bf16[128,2048]{1,0:T(8,128)(2,1)} custom-call(bf16[2,2,8,64,512]{4,3,2,1,0:T(8,128)(2,1)} %bitcast.23, s32[128,2]{1,0:T(8,128)} %copy.19.route_ref, f32[128,2]{1,0:T(8,128)} %copy.25.score_ref), custom_call_target="tpu_custom_call" | custom-call | flops 10000000000 | bytes 4194304 | tf_op jit(solution)/shard_map/return/pallas_call | solution.py:612
  102.2 0.0 collective-permute-done.1
  102.2 0.8 fusion.1
  102.9 1.9 %copy.28 = bf16[128,2048]{1,0:T(8,128)(2,1)} copy(bf16[128,2048]{1,0:T(8,128)(2,1)} %return.1) | data formatting | bytes 1048576
  (1 shorter events, 0.0 us)
Async XLA Ops:
  47.2 7.0 %copy-start.1 = (f32[128,2]{0,1:T(2,128)S(1)}, f32[128,2]{0,1:T(2,128)}, u32[]{:S(2)}) copy-start(f32[128,2]{0,1:T(2,128)} %param.30) | copy-start | bytes 3076
  52.3 15.1 %collective-permute-start = (bf16[2,64,2048]{2,1,0:T(8,128)(2,1)S(1)}, bf16[2,64,2048]{2,1,0:T(8,128)(2,1)S(1)}, u32[]{:S(2)}, u32[]{:S(2)}) collective-permute-start(bf16[2,64,2048]{2,1,0:T(8,128)(2,1)S(1)} %dynamic-slice_bitcast_fusion), channel_id=1, source_target_pairs={{0,1},{1,0},{2,3},{3,2},{4,5},{5,4},{6,7},{7,6},{8,9},{9,8},{10,11... | collective-permute-start | bytes 1572872 | tf_op jit(solution)/shard_map/ppermute | solution.py:480
  54.9 12.5 %copy-start = (bf16[256,2048]{1,0:T(8,128)(2,1)S(1)}, bf16[256,2048]{1,0:T(8,128)(2,1)}, u32[]{:S(2)}) copy-start(bf16[256,2048]{1,0:T(8,128)(2,1)} %project.1) | copy-start | bytes 3145732
  67.6 34.6 %collective-permute-start.1 = (bf16[1,64,2048]{2,1,0:T(8,128)(2,1)S(1)}, bf16[1,64,2048]{2,1,0:T(8,128)(2,1)S(1)}, u32[]{:S(2)}, u32[]{:S(2)}) collective-permute-start(bf16[1,64,2048]{2,1,0:T(8,128)(2,1)S(1)} %constant_dynamic-slice_fusion), channel_id=1, source_target_pairs={{0,2},{1,3},{2,0},{3,1},{4,6},{5,7},{6,4},{7,5},{8,10},{9,11},{10,... | collective-permute-start | bytes 786440 | tf_op jit(solution)/shard_map/ppermute | solution.py:480
